TPU v7x, 32 devices: a whole 2x2x4 slice. The times are simulated.
32 devices in a mesh: tp: 32 (over z, y, x, core).
Axes of the slice: x: 2, y: 2, z: 4, core: 2. Of those that a mesh axis runs over, the one named last changes fastest.
Arguments:
- tokens: bfloat16 [32, 8, 4096], P('tp'), may hold values from -6 to 6
- block_norm_gain: float32 [2, 4096], replicated, may hold values from 0.1 to 1.9
- receptance_weight: bfloat16 [2, 32, 4096, 64], P(None, 'tp'), may hold values from -0.09375 to 0.09375
- key_weight: bfloat16 [2, 32, 4096, 64], P(None, 'tp'), may hold values from -0.09375 to 0.09375
- value_weight: bfloat16 [2, 32, 4096, 64], P(None, 'tp'), may hold values from -0.09375 to 0.09375
- decay_weight: bfloat16 [2, 32, 4096, 64], P(None, 'tp'), may hold values from -0.09375 to 0.09375
- learning_rate_weight: bfloat16 [2, 32, 4096, 64], P(None, 'tp'), may hold values from -0.09375 to 0.09375
- gate_weight: bfloat16 [2, 32, 4096, 64], P(None, 'tp'), may hold values from -0.09375 to 0.09375
- decay_bias_fixed: float32 [2, 2048], replicated, may hold values from -5 to 2
- self_token_weight: float32 [2, 2048], replicated, may hold values from -1.5 to 1.5
- readout_norm_gain: float32 [2, 2048], replicated, may hold values from 0.1 to 1.9
- output_weight: bfloat16 [2, 32, 64, 4096], P(None, 'tp'), may hold values from -0.125 to 0.125
- state: float32 [2, 32, 256, 4096], P(None, 'tp'), may hold values from -3 to 3
Outputs:
- mixed: bfloat16 [32, 8, 4096], P('tp')
- new_state: float32 [2, 32, 256, 4096], P(None, 'tp')
All inputs are finite; a program needn't handle non-finite values.
Results may differ from a plain program's by a relative error of at most 0.018.
Values may be sent and summed in bfloat16 or wider, within the bound.
A program may use at most 128 MiB of HBM per device.

v0:
```python
import functools

import jax
import jax.numpy as jnp
from jax import lax
from jax.experimental import pallas as pl
from jax.experimental.pallas import tpu as pltpu
from jax.sharding import PartitionSpec as P

D = 4096


RMS_EPS = 1e-06
GROUP_EPS = 0.00064


def swapped(shard, axis, stride):
    return lax.ppermute(shard, axis, [(i, i ^ 1 << stride) for i in range(lax.axis_size(axis))])


def for_sending(shard):

    def short(part):
        return part.astype(jnp.bfloat16) if part.dtype == jnp.float32 else part

    return jax.tree.map(short, shard)


def recurrent_update(
    layer_state,
    receptance_vector,
    key_vector,
    value_vector,
    decay_logits,
    learning_rate_logits,
    gate_logits,
    decay_constant,
    self_term_scale,
    head_gain_slice,
):
    highest = lax.Precision.HIGHEST
    shrink = jnp.exp(-jnp.exp(-jax.nn.softplus(-(decay_constant + decay_logits)) - 0.5))
    rate = jax.nn.sigmoid(learning_rate_logits)
    normed = key_vector * lax.rsqrt(jnp.sum(key_vector * key_vector, -1, keepdims=True) + 1.0)
    removed = jnp.einsum("...ij,...j->...i", layer_state, normed, precision=highest)
    layer_state = (
        layer_state * shrink[..., None, :]
        - removed[..., :, None] * (normed * rate)[..., None, :]
        + value_vector[..., :, None] * (key_vector * rate)[..., None, :]
    )
    readout = jnp.einsum("...ij,...j->...i", layer_state, receptance_vector, precision=highest)
    center = jnp.mean(readout, -1, keepdims=True)
    spread = jnp.mean(jnp.square(readout - center), -1, keepdims=True)
    normed_output = (readout - center) * lax.rsqrt(spread + GROUP_EPS) * head_gain_slice
    self_term = (
        jnp.sum(receptance_vector * key_vector * self_term_scale, -1, keepdims=True) * value_vector
    )
    return (
        ((normed_output + self_term) * jax.nn.sigmoid(gate_logits)).astype(jnp.bfloat16),
        layer_state,
    )


def double_gather(piece, position, first_bit, count, mover):
    for offset in range(count):
        which_bit = first_bit + offset
        partner = mover(piece, which_bit)
        lower_self = position >> which_bit & 1 == 0
        piece = jnp.where(
            lower_self, jnp.concatenate([piece, partner], 0), jnp.concatenate([partner, piece], 0)
        )
    return piece


def halve_sum(members, position, first_bit, count, mover):
    for offset in reversed(range(count)):
        which_bit = first_bit + offset
        upper_self = position >> which_bit & 1 == 1
        sends = tuple(
            (
                jnp.where(
                    upper_self, member[: member.shape[0] // 2], member[member.shape[0] // 2 :]
                )
                for member in members
            )
        )
        keeps = tuple(
            (
                jnp.where(
                    upper_self, member[member.shape[0] // 2 :], member[: member.shape[0] // 2]
                )
                for member in members
            )
        )
        arrived = mover(sends, which_bit)
        members = tuple((kept + got for kept, got in zip(keeps, arrived)))
    return members


def on_device(
    tokens,
    block_norm_gain,
    receptance_weight,
    key_weight,
    value_weight,
    decay_weight,
    learning_rate_weight,
    gate_weight,
    decay_bias_fixed,
    self_token_weight,
    readout_norm_gain,
    output_weight,
    state,
):
    columns_dev = tokens.shape[2]
    row_blocks = D // columns_dev
    low_bits = row_blocks.bit_length() - 1
    head_count = lax.axis_size("tp") // row_blocks
    high_bits = head_count.bit_length() - 1
    position = lax.axis_index("tp")
    head_index = position // row_blocks
    row_block = position % row_blocks
    head_size = receptance_weight.shape[3]
    seq_tile = tokens.shape[1]
    move_rows = lambda payload, which_bit: swapped(payload, "tp", which_bit)
    move_proj = lambda payload, which_bit: swapped(payload, "tp", which_bit)
    move_outs = lambda payload, which_bit: jax.tree.map(
        lambda part, own: part.astype(own.dtype),
        swapped(for_sending(payload), "tp", which_bit),
        payload,
    )
    move_split = lambda payload, which_bit: jax.tree.map(
        lambda part, own: part.astype(own.dtype),
        swapped(for_sending(payload), "tp", which_bit),
        payload,
    )

    def mixer(columns, layer_index):
        gain_cols = lax.dynamic_slice_in_dim(
            block_norm_gain[layer_index], row_block * columns_dev, columns_dev
        )
        wide = columns.astype(jnp.float32)
        scaled = (wide * gain_cols).astype(jnp.bfloat16)
        squares = jnp.sum(wide * wide, axis=1)
        weights = jnp.concatenate(
            [
                receptance_weight[layer_index, 0],
                key_weight[layer_index, 0],
                value_weight[layer_index, 0],
                decay_weight[layer_index, 0],
                learning_rate_weight[layer_index, 0],
                gate_weight[layer_index, 0],
            ],
            axis=1,
        )
        partial_value = jnp.dot(scaled, weights, preferred_element_type=jnp.float32)
        summed, total_sq = halve_sum((partial_value, squares), position, 0, low_bits, move_proj)
        projected = summed * lax.rsqrt(total_sq / D + RMS_EPS)[:, None]
        output_pieces = jnp.split(projected, 6, axis=1)

        def head_columns(table):
            return lax.dynamic_slice_in_dim(table[layer_index], head_index * head_size, head_size)

        layer_state = state[layer_index, 0].reshape(-1, head_size, head_size)
        out_tile, layer_state = recurrent_update(
            layer_state,
            *output_pieces,
            head_columns(decay_bias_fixed),
            head_columns(self_token_weight),
            head_columns(readout_norm_gain)
        )
        out_all = double_gather(out_tile, position, 0, low_bits, move_outs)
        branch = jnp.dot(out_all, output_weight[layer_index, 0], preferred_element_type=jnp.float32)
        return (branch, layer_state.reshape(layer_state.shape[0], head_size * head_size))

    columns = double_gather(tokens[0], position, low_bits, high_bits, move_rows)
    first_branch, first_memory = mixer(columns, 0)
    (tile_sum,) = halve_sum((first_branch,), position, low_bits, high_bits, move_split)
    tile_one = (tokens[0].astype(jnp.float32) + tile_sum).astype(jnp.bfloat16)
    columns = double_gather(tile_one, position, low_bits, high_bits, move_rows)
    second_branch, second_memory = mixer(columns, 1)
    (tile_sum,) = halve_sum((second_branch,), position, low_bits, high_bits, move_split)
    resid_rows = lax.dynamic_slice_in_dim(columns, head_index * seq_tile, seq_tile, 0)
    mixed = (resid_rows.astype(jnp.float32) + tile_sum).astype(jnp.bfloat16)
    new_state = jnp.stack([first_memory, second_memory])[:, None]
    return (mixed[None], new_state)


class Place:
    def __init__(self, n):
        me = lax.axis_index("tp")
        self.n, self.planes = n, n // 8
        self.me = me
        self.c = me % 2
        self.x = (me // 2) % 2
        self.y = (me // 4) % 2
        self.z = me // 8
        self.sib = me + 1 - 2 * self.c
        self.xn = me + 2 * (1 - 2 * self.x)
        self.yn = me + 4 * (1 - 2 * self.y)
        self.far = [self.planes // 2] + [k for k in range(1, self.planes) if k != self.planes // 2]
        self.near = [k for k in self.far if k != self.planes // 2] + [self.planes // 2]

    def plane(self, k):
        return (self.z + k) % self.planes

    def zn(self, k):
        return self.plane(k) * 8 + self.me % 8

    def greet(self):
        barrier = pltpu.get_barrier_semaphore()
        others = [self.sib, self.xn, self.yn] + [self.zn(k) for k in self.far]
        for other in others:
            pl.semaphore_signal(
                barrier, inc=1, device_id=(other,), device_id_type=pl.DeviceIdType.MESH
            )
        pl.semaphore_wait(barrier, len(others))


def remote(src, dst, send, recv, to):
    return pltpu.make_async_remote_copy(
        src_ref=src,
        dst_ref=dst,
        send_sem=send,
        recv_sem=recv,
        device_id=(to,),
        device_id_type=pl.DeviceIdType.MESH,
    )


def gather_sends(n):
    planes = n // 8
    return (planes - 1) + 3 * planes + 4 * planes + 2 * planes


def gather_phase(at, own_ref, full_ref, send, recv_a, recv_b):
    half = own_ref.shape[1] // 2
    first, second = pl.ds(0, half), pl.ds(half, half)
    started = []

    def tile(p, y, x, c):
        return ((p * 2 + y) * 2 + x) * 2 + c

    def go(src, t, to, cols=None, recv=recv_a):
        dst = full_ref.at[t]
        if cols is not None:
            src, dst = src.at[:, cols], dst.at[:, cols]
        copy = remote(src, dst, send.at[len(started)], recv.at[t], to)
        copy.start()
        started.append(copy)

    def arrived(t, cols=None, recv=recv_a):
        dst = full_ref.at[t]
        if cols is not None:
            dst = dst.at[:, cols]
        remote(dst, dst, send.at[0], recv.at[t], at.sib).wait_recv()

    for k in at.near:
        go(own_ref, at.me, at.zn(k))
    go(own_ref, at.me, at.xn)
    go(own_ref, at.me, at.yn)
    go(own_ref, at.me, at.sib)
    full_ref[at.me] = own_ref[...]

    def spread(k):
        p = at.plane(k)
        t = tile(p, at.y, 1 - at.x, at.c)
        arrived(t)
        go(full_ref.at[t], t, at.yn, first, recv_a)
        go(full_ref.at[t], t, at.sib)
        t = tile(p, 1 - at.y, at.x, at.c)
        arrived(t)
        go(full_ref.at[t], t, at.xn, second, recv_b)
        go(full_ref.at[t], t, at.sib)

    def corner(k):
        t = tile(at.plane(k), 1 - at.y, 1 - at.x, at.c)
        arrived(t, first, recv_a)
        go(full_ref.at[t], t, at.sib, first, recv_a)
        arrived(t, second, recv_b)
        go(full_ref.at[t], t, at.sib, second, recv_b)

    order = [0] + at.near
    for step, k in enumerate(order):
        if step:
            t = at.zn(k)
            arrived(t)
            go(full_ref.at[t], t, at.xn)
            go(full_ref.at[t], t, at.yn)
            go(full_ref.at[t], t, at.sib)
        if step >= 1:
            spread(order[step - 1])
        if step >= 2:
            corner(order[step - 2])
    spread(order[-1])
    if len(order) > 1:
        corner(order[-2])
    corner(order[-1])
    for k in order:
        p = at.plane(k)
        for y in (at.y, 1 - at.y):
            for x in (at.x, 1 - at.x):
                t = tile(p, y, x, 1 - at.c)
                if y is not at.y and x is not at.x:
                    arrived(t, first, recv_a)
                    arrived(t, second, recv_b)
                else:
                    arrived(t)
    for copy in started:
        copy.wait_send()


def start_loads(layer, weights, joined_ref, load):
    head = weights[0].shape[2]
    loads = [
        pltpu.make_async_copy(w.at[layer, 0], joined_ref.at[pl.ds(i * head, head)], load.at[i])
        for i, w in enumerate(weights)
    ]
    for copy in loads:
        copy.start()
    return loads


def project_rows(layer, x_ref, gain_ref, w_ref, out_ref):
    columns = x_ref.shape[2]
    chunk = columns // 8
    acc, squares = None, None
    for at in range(0, columns, chunk):
        wide = x_ref[:, :, at : at + chunk].astype(jnp.float32).reshape(-1, chunk)
        scaled = (wide * gain_ref[layer : layer + 1, at : at + chunk]).astype(jnp.bfloat16)
        part = lax.dot_general(
            scaled,
            w_ref[:, at : at + chunk],
            (((1,), (1,)), ((), ())),
            preferred_element_type=jnp.float32,
        )
        square = wide * wide
        folded = square[:, :128]
        for lane in range(128, chunk, 128):
            folded = folded + square[:, lane : lane + 128]
        acc = part if acc is None else acc + part
        squares = folded if squares is None else squares + folded
    mean = jnp.sum(squares, axis=1, keepdims=True) / columns
    out_ref[...] = acc * lax.rsqrt(mean + RMS_EPS)


def gather_kernel(n, own_ref, gain_ref, *refs, layer):
    weights, (proj_ref, full_ref, joined_ref, load, *sems) = refs[:6], refs[6:]
    loads = start_loads(layer, weights, joined_ref, load)
    at = Place(n)
    at.greet()
    gather_phase(at, own_ref, full_ref, *sems)
    for copy in loads:
        copy.wait()
    project_rows(layer, full_ref, gain_ref, joined_ref, proj_ref)


def sum_scratch(n, rows, columns):
    planes, half = n // 8, columns // 2
    tiles = lambda count, width: pltpu.VMEM((count, rows, width), jnp.bfloat16)
    return [
        tiles(n // 2, columns),
        tiles(n // 2, columns),
        tiles(planes, half),
        tiles(planes, half),
        tiles(planes, columns),
        tiles(planes, columns),
        tiles(planes, columns),
        tiles(planes, columns),
        pltpu.SemaphoreType.DMA((6 * planes,)),
        pltpu.SemaphoreType.DMA((6 * planes,)),
    ]


def sum_phase(at, part_ref, scratch):
    sib, acc, in_a, in_b, in_x, in_y, out_z, in_z, send, recv = scratch
    planes = at.planes
    half = part_ref.shape[3] // 2
    first, second = pl.ds(0, half), pl.ds(half, half)
    order = at.far + [0]
    started = []

    def go(src, dst, kind, k, to):
        copy = remote(src, dst, send.at[kind * planes + k], recv.at[kind * planes + k], to)
        copy.start()
        started.append(copy)

    def arrived(dst, kind, k):
        slot = kind * planes + k
        remote(dst, dst, send.at[slot], recv.at[slot], at.sib).wait_recv()

    def f32(v):
        return v.astype(jnp.float32)

    def chunk(p, y, x):
        return (p * 2 + y) * 2 + x

    for k in order:
        block = pl.ds(at.plane(k) * 4, 4)
        go(part_ref.at[block, 1 - at.c], sib.at[block], 0, k, at.sib)
    for k in order:
        p = at.plane(k)
        block = pl.ds(p * 4, 4)
        arrived(sib.at[block], 0, k)
        for y, x in ((1 - at.y, 1 - at.x), (at.y, 1 - at.x), (1 - at.y, at.x), (at.y, at.x)):
            q = chunk(p, y, x)
            acc[q] = (f32(part_ref[q, at.c]) + f32(sib[q])).astype(jnp.bfloat16)
            if y is not at.y and x is not at.x:
                go(acc.at[q, :, first], in_a.at[k], 1, k, at.yn)
                go(acc.at[q, :, second], in_b.at[k], 2, k, at.xn)
    for k in order:
        p = at.plane(k)
        q = chunk(p, at.y, 1 - at.x)
        arrived(in_a.at[k], 1, k)
        acc[q, :, first] = (f32(acc[q, :, first]) + f32(in_a[k])).astype(jnp.bfloat16)
        go(acc.at[q], in_x.at[k], 3, k, at.xn)
        q = chunk(p, 1 - at.y, at.x)
        arrived(in_b.at[k], 2, k)
        acc[q, :, second] = (f32(acc[q, :, second]) + f32(in_b[k])).astype(jnp.bfloat16)
        go(acc.at[q], in_y.at[k], 4, k, at.yn)
    total = None
    for k in order:
        arrived(in_x.at[k], 3, k)
        arrived(in_y.at[k], 4, k)
        plane = f32(acc[chunk(at.plane(k), at.y, at.x)]) + f32(in_x[k]) + f32(in_y[k])
        if k:
            out_z[k] = plane.astype(jnp.bfloat16)
            go(out_z.at[k], in_z.at[k], 5, k, at.zn(k))
        else:
            total = plane
    for k in at.near:
        arrived(in_z.at[k], 5, k)
        total = total + f32(in_z[k])
    for copy in started:
        copy.wait_send()
    return total


def middle_kernel(n, part_ref, own_ref, gain_ref, *refs, layer):
    weights, (proj_ref, next_ref, full_ref, joined_ref, load, *rest) = refs[:6], refs[6:]
    loads = start_loads(layer, weights, joined_ref, load)
    at = Place(n)
    at.greet()
    total = sum_phase(at, part_ref, rest[3:])
    next_ref[...] = (own_ref[...].astype(jnp.float32) + total).astype(jnp.bfloat16)
    gather_phase(at, next_ref, full_ref, *rest[:3])
    for copy in loads:
        copy.wait()
    project_rows(layer, full_ref, gain_ref, joined_ref, proj_ref)


def last_kernel(n, part_ref, own_ref, next_ref, *scratch):
    at = Place(n)
    at.greet()
    total = sum_phase(at, part_ref, scratch)
    next_ref[...] = (own_ref[...].astype(jnp.float32) + total).astype(jnp.bfloat16)


def comm_call(kernel, n, collective_id, out_shape, scratch_shapes, *operands):
    vmem, hbm = [pl.BlockSpec(memory_space=m) for m in (pltpu.VMEM, pltpu.HBM)]
    return pl.pallas_call(
        functools.partial(kernel, n),
        out_shape=out_shape,
        in_specs=[hbm if o.ndim == 4 and o.shape[0] != n // 2 else vmem for o in operands],
        out_specs=jax.tree.map(lambda _: vmem, out_shape),
        scratch_shapes=scratch_shapes,
        compiler_params=pltpu.CompilerParams(
            collective_id=collective_id, has_side_effects=True, vmem_limit_bytes=(14 if collective_id == 2 else 58) << 20
        ),
        cost_estimate=pl.CostEstimate(flops=0, bytes_accessed=50 << 20, transcendentals=0),
    )(*operands)


def gather_scratch(n):
    return [
        pltpu.SemaphoreType.DMA((gather_sends(n),)),
        pltpu.SemaphoreType.DMA((n,)),
        pltpu.SemaphoreType.DMA((n,)),
    ]


def lanes(v, times):
    return jnp.concatenate([v] * times, axis=1)


def own_head(ref, layer, head):
    position = lax.axis_index("tp")
    start = pl.multiple_of(position // 2 * (2 * head), 2 * head)
    pair = ref[layer : layer + 1, pl.ds(start, 2 * head)]
    return jnp.where(position % 2 == 0, pair[:, :head], pair[:, head:])


def state_kernel(
    layer, proj_ref, state_ref, bias_ref, self_ref, gain_ref, w_ref, spread_ref, *refs
):
    part_ref, new_ref = refs[-2:]
    head = w_ref.shape[2]
    bias, self_w, ro_gain = [own_head(t, layer, head) for t in (bias_ref, self_ref, gain_ref)]
    rows, flat = state_ref.shape[2:]
    chunk = 8 * head
    r, k, v, p, q, g = [proj_ref[:, i * head : (i + 1) * head] for i in range(6)]
    decay = jnp.exp(-jax.nn.sigmoid(bias + p) * jnp.exp(jnp.float32(-0.5)))
    rate = jax.nn.sigmoid(q)
    kn = k * lax.rsqrt(jnp.sum(k * k, axis=1, keepdims=True) + 1.0)
    taken, added = kn * rate, k * rate
    kn_w, u_w = lanes(kn, chunk // head), lanes(decay * r, chunk // head)
    sums = jnp.zeros((2 * rows, head), jnp.float32)
    for at in range(0, flat, chunk):
        s = state_ref[0, 0, :, at : at + chunk]
        both = jnp.concatenate([s * kn_w, s * u_w], axis=0).astype(jnp.bfloat16)
        sums += lax.dot_general(
            both,
            spread_ref[:head, at : at + chunk],
            (((1,), (1,)), ((), ())),
            preferred_element_type=jnp.float32,
        )
    removed, read = sums[:rows], sums[rows:]
    read = (
        read
        - removed * jnp.sum(taken * r, axis=1, keepdims=True)
        + v * jnp.sum(added * r, axis=1, keepdims=True)
    )
    center = jnp.mean(read, axis=1, keepdims=True)
    off = read - center
    spread = jnp.mean(off * off, axis=1, keepdims=True)
    normed = off * lax.rsqrt(spread + GROUP_EPS) * ro_gain
    own_term = jnp.sum(r * k * self_w, axis=1, keepdims=True) * v
    o = ((normed + own_term) * jax.nn.sigmoid(g)).astype(jnp.bfloat16)

    pair = jnp.concatenate([removed, v], axis=0)
    high = pair.astype(jnp.bfloat16)
    low = (pair - high.astype(jnp.float32)).astype(jnp.bfloat16)
    pair = jnp.concatenate([high, low], axis=1)
    decay_w, taken_w, added_w = [lanes(t, chunk // head) for t in (decay, taken, added)]
    columns = w_ref.shape[3]
    for at in range(0, columns, chunk):
        part = jnp.dot(o, w_ref[0, 0, :, at : at + chunk], preferred_element_type=jnp.float32)
        part = part.reshape(part_ref.shape[:3] + (chunk,))
        part_ref[:, :, :, at : at + chunk] = part.astype(jnp.bfloat16)
    for at in range(0, flat, chunk):
        wide = jnp.dot(pair, spread_ref[:, at : at + chunk], preferred_element_type=jnp.float32)
        new_ref[0, 0, :, at : at + chunk] = (
            state_ref[0, 0, :, at : at + chunk] * decay_w
            - wide[:rows] * taken_w
            + wide[rows:] * added_w
        )


def state_step(n, tile_rows, proj, state, tables, w_out, spread, layer, earlier):
    seqs, flat = state.shape[2:]
    head, columns = w_out.shape[2:]
    rows = seqs // 2
    state_spec = pl.BlockSpec((1, 1, rows, flat), lambda i: (layer, 0, i, 0))
    whole = lambda a: pl.BlockSpec(a.shape, lambda i: (0,) * a.ndim)
    operands = [proj, state, *tables, w_out, spread]
    in_specs = [
        pl.BlockSpec((rows, proj.shape[1]), lambda i: (i, 0)),
        state_spec,
        *[whole(t) for t in tables],
        pl.BlockSpec((1, 1, head, columns), lambda i: (layer, 0, 0, 0)),
        whole(spread),
    ]
    if earlier is not None:
        operands.append(earlier)
        in_specs.append(pl.BlockSpec(memory_space=pl.ANY))
    per = rows // tile_rows // 2
    return pl.pallas_call(
        functools.partial(state_kernel, layer),
        grid=(2,),
        in_specs=in_specs,
        out_specs=(
            pl.BlockSpec((per, 2, tile_rows, columns), lambda i: (i, 0, 0, 0)),
            state_spec,
        ),
        out_shape=(
            jax.ShapeDtypeStruct((n // 2, 2, tile_rows, columns), jnp.bfloat16),
            jax.ShapeDtypeStruct(state.shape, jnp.float32),
        ),
        input_output_aliases={} if earlier is None else {7: 1},
        compiler_params=pltpu.CompilerParams(vmem_limit_bytes=48 << 20),
    )(*operands)


def on_device_fast(n, *args):
    tokens, gain, wr, wk, wv, wd, wq, wg, bias, self_w, ro_gain, w_out, state = args
    weights = [jnp.swapaxes(w, 2, 3) for w in (wr, wk, wv, wd, wq, wg)]
    own = tokens[0]
    rows, columns = own.shape
    head = wr.shape[3]
    flat = state.shape[3]
    proj_shape = jax.ShapeDtypeStruct((n * rows, 6 * head), jnp.float32)
    gather_space = [
        pltpu.VMEM((n, rows, columns), own.dtype),
        pltpu.VMEM((6 * head, columns), wr.dtype),
        pltpu.SemaphoreType.DMA((6,)),
    ] + gather_scratch(n)
    own_shape = jax.ShapeDtypeStruct(own.shape, own.dtype)
    tables = (bias, self_w, ro_gain)
    value_of = jnp.arange(flat) // head
    spread = (jnp.arange(2 * head)[:, None] % head == value_of[None]).astype(jnp.bfloat16)

    def mixer(proj, layer, earlier):
        return state_step(n, rows, proj, state, tables, w_out, spread, layer, earlier)

    first = functools.partial(gather_kernel, layer=0)
    proj = comm_call(first, n, 0, proj_shape, gather_space, own, gain, *weights)
    part, new_state = mixer(proj, 0, None)
    proj, own = comm_call(
        functools.partial(middle_kernel, layer=1),
        n,
        1,
        (proj_shape, own_shape),
        gather_space + sum_scratch(n, rows, columns),
        part,
        own,
        gain,
        *weights,
    )
    part, new_state = mixer(proj, 1, new_state)
    mixed = comm_call(last_kernel, n, 2, own_shape, sum_scratch(n, rows, columns), part, own)
    return mixed[None], new_state


def pick(n, *args):
    one_block = args[0].shape[2] == args[1].shape[1]
    if one_block and n % 16 == 0 and 2 * args[2].shape[3] % 128 == 0:
        return on_device_fast(n, *args)
    return on_device(*args)


def solution(mesh):
    return jax.shard_map(
        functools.partial(pick, mesh.shape["tp"]),
        mesh=mesh,
        in_specs=(
            P("tp", None, None),
            P(),
            P(None, "tp", None, None),
            P(None, "tp", None, None),
            P(None, "tp", None, None),
            P(None, "tp", None, None),
            P(None, "tp", None, None),
            P(None, "tp", None, None),
            P(),
            P(),
            P(),
            P(None, "tp", None, None),
            P(None, "tp", None, None),
        ),
        out_specs=(P("tp", None, None), P(None, "tp", None, None)),
        check_vma=False,
    )
```

profile of v0, /device:TPU:0, one launch (start us, length us, event | category | flops | bytes accessed | tf_op | source)
XLA Modules:
  0.0 106.2 jit_solution(4499699834130908464)
XLA Ops:
  0.7 0.0 copy-start
  0.7 0.0 copy-start.5
  0.7 0.0 copy-start.6
  0.7 0.0 copy-start.7
  0.7 25.0 %shard_map.140.proj_ref = f32[256,384]{1,0:T(8,128)} custom-call(bf16[8,4096]{1,0:T(8,128)(2,1)} %bitcast.21, f32[2,4096]{1,0:T(2,128)} %gain_ref.6, bf16[2,1,64,4096]{3,2,1,0:T(8,128)(2,1)} %bitcast.9, bf16[2,1,64,4096]{3,2,1,0:T(8,128)(2,1)} %bitcast.11, bf16[2,1,64,4096]{3,2,1,0:T(8,128)(2,1)} %bitcast.13, bf16[2,1,64,4096]{3,2,1,0:T(8,128)(2,1)} %bitcast.15, ...), custom_call_target="tpu_custom_call" | custom-call | bytes 52428800 | tf_op jit(solution)/shard_map/pallas_call | solution.py:461
  25.7 0.3 compare_convert_fusion.spread_ref
  25.9 0.0 copy-done
  25.9 0.0 copy-done.5
  26.0 0.0 copy-done.6
  26.0 0.0 copy-done.7
  26.0 0.0 copy-start.2
  26.0 1.0 copy-done.2
  27.0 9.3 %shard_map.141 = (bf16[16,2,8,4096]{3,2,1,0:T(8,128)(2,1)S(1)}, f32[2,1,256,4096]{3,2,1,0:T(8,128)}) custom-call(f32[256,384]{1,0:T(8,128)S(1)} %copy-done.2, f32[2,1,256,4096]{3,2,1,0:T(8,128)} %state_ref.3, f32[2,2048]{1,0:T(2,128)S(1)} %copy-done.5, f32[2,2048]{1,0:T(2,128)S(1)} %copy-done.6, f32[2,2048]{1,0:T(2,128)S(1)} %copy-done.7, ...), custom_call_target="tpu_custom_call" | custom-call | tf_op jit(solution)/shard_map/pallas_call | solution.py:567
  36.2 0.0 copy-start.1
  36.2 1.3 %copy-done.1 = bf16[16,2,8,4096]{3,2,1,0:T(8,128)(2,1)} copy-done((bf16[16,2,8,4096]{3,2,1,0:T(8,128)(2,1)}, bf16[16,2,8,4096]{3,2,1,0:T(8,128)(2,1)S(1)}, u32[]{:S(2)}) %copy-start.1) | copy-done | bytes 2097176
  37.6 39.3 %shard_map.142 = (f32[256,384]{1,0:T(8,128)}, bf16[8,4096]{1,0:T(8,128)(2,1)}) custom-call(bf16[16,2,8,4096]{3,2,1,0:T(8,128)(2,1)} %copy-done.1, bf16[8,4096]{1,0:T(8,128)(2,1)} %bitcast.22, f32[2,4096]{1,0:T(2,128)} %gain_ref.6, bf16[2,1,64,4096]{3,2,1,0:T(8,128)(2,1)} %bitcast.10, bf16[2,1,64,4096]{3,2,1,0:T(8,128)(2,1)} %bitcast.12, ...), custom_call_target="tpu_custom_call" | custom-call | bytes 52428800 | tf_op jit(solution)/shard_map/pallas_call | solution.py:461
  76.8 0.0 copy-start.3
  76.9 1.0 copy-done.3
  77.8 0.0 copy-start.4
  77.8 9.3 %shard_map.143 = (bf16[16,2,8,4096]{3,2,1,0:T(8,128)(2,1)S(1)}, f32[2,1,256,4096]{3,2,1,0:T(8,128)}) custom-call(f32[256,384]{1,0:T(8,128)S(1)} %copy-done.3, f32[2,1,256,4096]{3,2,1,0:T(8,128)} %state_ref.3, f32[2,2048]{1,0:T(2,128)S(1)} %copy-done.5, f32[2,2048]{1,0:T(2,128)S(1)} %copy-done.6, ...), custom_call_target="tpu_custom_call", output_to_operand_aliasing={{1}: (7, {})} | custom-call | tf_op jit(solution)/shard_map/pallas_call | solution.py:567
  87.2 0.0 copy-done.4
  87.2 18.4 %shard_map.144 = bf16[8,4096]{1,0:T(8,128)(2,1)S(1)} custom-call(bf16[16,2,8,4096]{3,2,1,0:T(8,128)(2,1)S(1)} %get-tuple-element.11.part_ref, bf16[8,4096]{1,0:T(8,128)(2,1)S(1)} %copy-done.4), custom_call_target="tpu_custom_call" | custom-call | bytes 52428800 | tf_op jit(solution)/shard_map/pallas_call | solution.py:461
  105.6 0.6 copy.18
  (2 shorter events, 0.0 us)
Async XLA Ops:
  0.7 25.3 %copy-start = (bf16[2,1,64,4096]{3,2,1,0:T(8,128)(2,1)S(1)}, bf16[2,1,64,4096]{3,2,1,0:T(8,128)(2,1)}, u32[]{:S(2)}) copy-start(bf16[2,1,64,4096]{3,2,1,0:T(8,128)(2,1)} %w_ref.3) | copy-start | bytes 3145732
  0.7 25.3 %copy-start.5 = (f32[2,2048]{1,0:T(2,128)S(1)}, f32[2,2048]{1,0:T(2,128)}, u32[]{:S(2)}) copy-start(f32[2,2048]{1,0:T(2,128)} %bias_ref.3) | copy-start | bytes 49156
  0.7 25.3 %copy-start.6 = (f32[2,2048]{1,0:T(2,128)S(1)}, f32[2,2048]{1,0:T(2,128)}, u32[]{:S(2)}) copy-start(f32[2,2048]{1,0:T(2,128)} %self_ref.3) | copy-start | bytes 49156
  0.7 25.3 %copy-start.7 = (f32[2,2048]{1,0:T(2,128)S(1)}, f32[2,2048]{1,0:T(2,128)}, u32[]{:S(2)}) copy-start(f32[2,2048]{1,0:T(2,128)} %gain_ref.7) | copy-start | bytes 49156
  26.0 1.0 copy-start.2
  36.2 1.3 %copy-start.1 = (bf16[16,2,8,4096]{3,2,1,0:T(8,128)(2,1)}, bf16[16,2,8,4096]{3,2,1,0:T(8,128)(2,1)S(1)}, u32[]{:S(2)}) copy-start(bf16[16,2,8,4096]{3,2,1,0:T(8,128)(2,1)S(1)} %get-tuple-element.8.part_ref) | copy-start | bytes 6291460
  76.8 1.0 copy-start.3
  77.8 9.3 %copy-start.4 = (bf16[8,4096]{1,0:T(8,128)(2,1)S(1)}, bf16[8,4096]{1,0:T(8,128)(2,1)}, u32[]{:S(2)}) copy-start(bf16[8,4096]{1,0:T(8,128)(2,1)} %get-tuple-element.12.own_ref) | copy-start | bytes 196612
where the time goes:
time: 106 us
  Pallas kernels  101 us (95%)
  local copies, waits for them, and re-layouts  3.97 us (4%)
    pallas_call x3, Pallas kernels, comm_call(): pl.pallas_call(functools.partial(kernel, n), out_shape=out_shape, in_spec...  82.7 us
    pallas_call x2, Pallas kernels, state_step(): pl.pallas_call(functools.partial(state_kernel, layer), grid=(2,), in_spec...  18.6 us
    unnamed x17, local copies, waits for them, and re-layouts  3.97 us

commit v1 on v0

v1 whole, which is shorter than its diff:
```python
import functools

import jax
import jax.numpy as jnp
from jax import lax
from jax.experimental import pallas as pl
from jax.experimental.pallas import tpu as pltpu
from jax.sharding import PartitionSpec as P

D = 4096


RMS_EPS = 1e-06
GROUP_EPS = 0.00064


def swapped(shard, axis, stride):
    return lax.ppermute(shard, axis, [(i, i ^ 1 << stride) for i in range(lax.axis_size(axis))])


def for_sending(shard):

    def short(part):
        return part.astype(jnp.bfloat16) if part.dtype == jnp.float32 else part

    return jax.tree.map(short, shard)


def recurrent_update(
    layer_state,
    receptance_vector,
    key_vector,
    value_vector,
    decay_logits,
    learning_rate_logits,
    gate_logits,
    decay_constant,
    self_term_scale,
    head_gain_slice,
):
    highest = lax.Precision.HIGHEST
    shrink = jnp.exp(-jnp.exp(-jax.nn.softplus(-(decay_constant + decay_logits)) - 0.5))
    rate = jax.nn.sigmoid(learning_rate_logits)
    normed = key_vector * lax.rsqrt(jnp.sum(key_vector * key_vector, -1, keepdims=True) + 1.0)
    removed = jnp.einsum("...ij,...j->...i", layer_state, normed, precision=highest)
    layer_state = (
        layer_state * shrink[..., None, :]
        - removed[..., :, None] * (normed * rate)[..., None, :]
        + value_vector[..., :, None] * (key_vector * rate)[..., None, :]
    )
    readout = jnp.einsum("...ij,...j->...i", layer_state, receptance_vector, precision=highest)
    center = jnp.mean(readout, -1, keepdims=True)
    spread = jnp.mean(jnp.square(readout - center), -1, keepdims=True)
    normed_output = (readout - center) * lax.rsqrt(spread + GROUP_EPS) * head_gain_slice
    self_term = (
        jnp.sum(receptance_vector * key_vector * self_term_scale, -1, keepdims=True) * value_vector
    )
    return (
        ((normed_output + self_term) * jax.nn.sigmoid(gate_logits)).astype(jnp.bfloat16),
        layer_state,
    )


def double_gather(piece, position, first_bit, count, mover):
    for offset in range(count):
        which_bit = first_bit + offset
        partner = mover(piece, which_bit)
        lower_self = position >> which_bit & 1 == 0
        piece = jnp.where(
            lower_self, jnp.concatenate([piece, partner], 0), jnp.concatenate([partner, piece], 0)
        )
    return piece


def halve_sum(members, position, first_bit, count, mover):
    for offset in reversed(range(count)):
        which_bit = first_bit + offset
        upper_self = position >> which_bit & 1 == 1
        sends = tuple(
            (
                jnp.where(
                    upper_self, member[: member.shape[0] // 2], member[member.shape[0] // 2 :]
                )
                for member in members
            )
        )
        keeps = tuple(
            (
                jnp.where(
                    upper_self, member[member.shape[0] // 2 :], member[: member.shape[0] // 2]
                )
                for member in members
            )
        )
        arrived = mover(sends, which_bit)
        members = tuple((kept + got for kept, got in zip(keeps, arrived)))
    return members


def on_device(
    tokens,
    block_norm_gain,
    receptance_weight,
    key_weight,
    value_weight,
    decay_weight,
    learning_rate_weight,
    gate_weight,
    decay_bias_fixed,
    self_token_weight,
    readout_norm_gain,
    output_weight,
    state,
):
    columns_dev = tokens.shape[2]
    row_blocks = D // columns_dev
    low_bits = row_blocks.bit_length() - 1
    head_count = lax.axis_size("tp") // row_blocks
    high_bits = head_count.bit_length() - 1
    position = lax.axis_index("tp")
    head_index = position // row_blocks
    row_block = position % row_blocks
    head_size = receptance_weight.shape[3]
    seq_tile = tokens.shape[1]
    move_rows = lambda payload, which_bit: swapped(payload, "tp", which_bit)
    move_proj = lambda payload, which_bit: swapped(payload, "tp", which_bit)
    move_outs = lambda payload, which_bit: jax.tree.map(
        lambda part, own: part.astype(own.dtype),
        swapped(for_sending(payload), "tp", which_bit),
        payload,
    )
    move_split = lambda payload, which_bit: jax.tree.map(
        lambda part, own: part.astype(own.dtype),
        swapped(for_sending(payload), "tp", which_bit),
        payload,
    )

    def mixer(columns, layer_index):
        gain_cols = lax.dynamic_slice_in_dim(
            block_norm_gain[layer_index], row_block * columns_dev, columns_dev
        )
        wide = columns.astype(jnp.float32)
        scaled = (wide * gain_cols).astype(jnp.bfloat16)
        squares = jnp.sum(wide * wide, axis=1)
        weights = jnp.concatenate(
            [
                receptance_weight[layer_index, 0],
                key_weight[layer_index, 0],
                value_weight[layer_index, 0],
                decay_weight[layer_index, 0],
                learning_rate_weight[layer_index, 0],
                gate_weight[layer_index, 0],
            ],
            axis=1,
        )
        partial_value = jnp.dot(scaled, weights, preferred_element_type=jnp.float32)
        summed, total_sq = halve_sum((partial_value, squares), position, 0, low_bits, move_proj)
        projected = summed * lax.rsqrt(total_sq / D + RMS_EPS)[:, None]
        output_pieces = jnp.split(projected, 6, axis=1)

        def head_columns(table):
            return lax.dynamic_slice_in_dim(table[layer_index], head_index * head_size, head_size)

        layer_state = state[layer_index, 0].reshape(-1, head_size, head_size)
        out_tile, layer_state = recurrent_update(
            layer_state,
            *output_pieces,
            head_columns(decay_bias_fixed),
            head_columns(self_token_weight),
            head_columns(readout_norm_gain)
        )
        out_all = double_gather(out_tile, position, 0, low_bits, move_outs)
        branch = jnp.dot(out_all, output_weight[layer_index, 0], preferred_element_type=jnp.float32)
        return (branch, layer_state.reshape(layer_state.shape[0], head_size * head_size))

    columns = double_gather(tokens[0], position, low_bits, high_bits, move_rows)
    first_branch, first_memory = mixer(columns, 0)
    (tile_sum,) = halve_sum((first_branch,), position, low_bits, high_bits, move_split)
    tile_one = (tokens[0].astype(jnp.float32) + tile_sum).astype(jnp.bfloat16)
    columns = double_gather(tile_one, position, low_bits, high_bits, move_rows)
    second_branch, second_memory = mixer(columns, 1)
    (tile_sum,) = halve_sum((second_branch,), position, low_bits, high_bits, move_split)
    resid_rows = lax.dynamic_slice_in_dim(columns, head_index * seq_tile, seq_tile, 0)
    mixed = (resid_rows.astype(jnp.float32) + tile_sum).astype(jnp.bfloat16)
    new_state = jnp.stack([first_memory, second_memory])[:, None]
    return (mixed[None], new_state)


class Place:
    def __init__(self, n):
        me = lax.axis_index("tp")
        self.n, self.planes = n, n // 8
        self.me = me
        self.i = me % 8
        self.c = me % 2
        self.x = (me // 2) % 2
        self.y = (me // 4) % 2
        self.z = me // 8
        self.sib = self.peer(0, 0, 1)
        self.xn = self.peer(0, 1, 0)
        self.yn = self.peer(1, 0, 0)
        flips = [(1, 1, 0), (1, 1, 1), (1, 0, 0), (1, 0, 1), (0, 1, 0), (0, 1, 1), (0, 0, 1)]
        self.others = [self.peer(*f) for f in flips]
        half = self.planes // 2
        self.near = [k for k in range(1, self.planes) if k != half] + [half]

    def peer(self, dy, dx, dc):
        flip = lambda v, d: 1 - v if d else v
        return self.tile(self.z, flip(self.y, dy), flip(self.x, dx), flip(self.c, dc))

    def tile(self, p, y, x, c):
        return ((p * 2 + y) * 2 + x) * 2 + c

    def plane(self, k):
        return (self.z + k) % self.planes

    def zn(self, k):
        return self.plane(k) * 8 + self.i

    def greet(self):
        barrier = pltpu.get_barrier_semaphore()
        others = self.others + [self.zn(k) for k in self.near]
        for other in others:
            pl.semaphore_signal(
                barrier, inc=1, device_id=(other,), device_id_type=pl.DeviceIdType.MESH
            )
        pl.semaphore_wait(barrier, len(others))


def remote(src, dst, send, recv, to):
    return pltpu.make_async_remote_copy(
        src_ref=src,
        dst_ref=dst,
        send_sem=send,
        recv_sem=recv,
        device_id=(to,),
        device_id_type=pl.DeviceIdType.MESH,
    )


def gather_sends(n):
    planes = n // 8
    return (planes - 1) + 3 * planes + 4 * planes + 2 * planes


class Gather:
    def __init__(self, at, own_ref, full_ref, send, recv_a, recv_b):
        self.at, self.own, self.full = at, own_ref, full_ref
        self.send, self.recv_a, self.recv_b = send, recv_a, recv_b
        half = full_ref.shape[2] // 2
        self.first, self.second = pl.ds(0, half), pl.ds(half, half)
        self.started = []
        self.order = [0] + at.near

    def go(self, src, t, to, cols=None, recv=None):
        dst = self.full.at[t]
        if cols is not None:
            src, dst = src.at[:, cols], dst.at[:, cols]
        recv = self.recv_a if recv is None else recv
        copy = remote(src, dst, self.send.at[len(self.started)], recv.at[t], to)
        copy.start()
        self.started.append(copy)

    def arrived(self, t, cols=None, recv=None):
        dst = self.full.at[t]
        if cols is not None:
            dst = dst.at[:, cols]
        recv = self.recv_a if recv is None else recv
        remote(dst, dst, self.send.at[0], recv.at[t], self.at.sib).wait_recv()

    def start(self):
        at = self.at
        for k in at.near:
            self.go(self.own, at.me, at.zn(k))
        self.go(self.own, at.me, at.xn)
        self.go(self.own, at.me, at.yn)
        self.go(self.own, at.me, at.sib)

    def column(self, k):
        at = self.at
        t = at.zn(k)
        self.arrived(t)
        for to in (at.xn, at.yn, at.sib):
            self.go(self.full.at[t], t, to)

    def spread(self, k):
        at = self.at
        p = at.plane(k)
        t = at.tile(p, at.y, 1 - at.x, at.c)
        self.arrived(t)
        self.go(self.full.at[t], t, at.yn, self.first, self.recv_a)
        self.go(self.full.at[t], t, at.sib)
        t = at.tile(p, 1 - at.y, at.x, at.c)
        self.arrived(t)
        self.go(self.full.at[t], t, at.xn, self.second, self.recv_b)
        self.go(self.full.at[t], t, at.sib)

    def corner(self, k):
        at = self.at
        t = at.tile(at.plane(k), 1 - at.y, 1 - at.x, at.c)
        self.arrived(t, self.first, self.recv_a)
        self.go(self.full.at[t], t, at.sib, self.first, self.recv_a)
        self.arrived(t, self.second, self.recv_b)
        self.go(self.full.at[t], t, at.sib, self.second, self.recv_b)

    def finish(self, k):
        at = self.at
        p = at.plane(k)
        for y in (at.y, 1 - at.y):
            for x in (at.x, 1 - at.x):
                t = at.tile(p, y, x, 1 - at.c)
                if y is not at.y and x is not at.x:
                    self.arrived(t, self.first, self.recv_a)
                    self.arrived(t, self.second, self.recv_b)
                else:
                    self.arrived(t)

    def run(self, batch):
        order = self.order
        for step, k in enumerate(order):
            if step:
                self.column(k)
                self.spread(order[step - 1])
            if step >= 2:
                self.corner(order[step - 2])
        self.spread(order[-1])
        if len(order) > 1:
            self.corner(order[-2])
        self.corner(order[-1])
        for k in order:
            self.finish(k)
            batch(k)

    def drain(self):
        for copy in self.started:
            copy.wait_send()


def lanes(v, times):
    return jnp.concatenate([v] * times, axis=1)


def own_head(ref, layer, head):
    position = lax.axis_index("tp")
    start = pl.multiple_of(position // 2 * (2 * head), 2 * head)
    pair = ref[layer : layer + 1, pl.ds(start, 2 * head)]
    return jnp.where(position % 2 == 0, pair[:, :head], pair[:, head:])


def project(layer, read, columns, gain_ref, w_ref):
    chunk = columns // 8
    acc, squares = None, None
    for j in range(8):
        wide = read(j).astype(jnp.float32)
        cols = slice(j * chunk, (j + 1) * chunk)
        scaled = (wide * gain_ref[layer : layer + 1, cols]).astype(jnp.bfloat16)
        part = lax.dot_general(
            scaled,
            w_ref[layer, :, cols],
            (((1,), (1,)), ((), ())),
            preferred_element_type=jnp.float32,
        )
        square = wide * wide
        folded = square[:, :128]
        for lane in range(128, chunk, 128):
            folded = folded + square[:, lane : lane + 128]
        acc = part if acc is None else acc + part
        squares = folded if squares is None else squares + folded
    mean = jnp.sum(squares, axis=1, keepdims=True) / columns
    return acc * lax.rsqrt(mean + RMS_EPS)


def read_state(proj, heads, state_ref, at_rows, spread_ref):
    bias, self_w, ro_gain = heads
    head = bias.shape[1]
    rows = proj.shape[0]
    flat = state_ref.shape[1]
    chunk = 8 * head
    r, k, v, p, q, g = [proj[:, i * head : (i + 1) * head] for i in range(6)]
    decay = jnp.exp(-jax.nn.sigmoid(bias + p) * jnp.exp(jnp.float32(-0.5)))
    rate = jax.nn.sigmoid(q)
    kn = k * lax.rsqrt(jnp.sum(k * k, axis=1, keepdims=True) + 1.0)
    taken, added = kn * rate, k * rate
    kn_w, u_w = lanes(kn, chunk // head), lanes(decay * r, chunk // head)
    sums = jnp.zeros((2 * rows, head), jnp.float32)
    for at in range(0, flat, chunk):
        s = state_ref[at_rows, at : at + chunk]
        both = jnp.concatenate([s * kn_w, s * u_w], axis=0).astype(jnp.bfloat16)
        sums += lax.dot_general(
            both,
            spread_ref[:head, at : at + chunk],
            (((1,), (1,)), ((), ())),
            preferred_element_type=jnp.float32,
        )
    removed, read = sums[:rows], sums[rows:]
    read = (
        read
        - removed * jnp.sum(taken * r, axis=1, keepdims=True)
        + v * jnp.sum(added * r, axis=1, keepdims=True)
    )
    center = jnp.mean(read, axis=1, keepdims=True)
    off = read - center
    spread = jnp.mean(off * off, axis=1, keepdims=True)
    normed = off * lax.rsqrt(spread + GROUP_EPS) * ro_gain
    own_term = jnp.sum(r * k * self_w, axis=1, keepdims=True) * v
    o = (normed + own_term) * jax.nn.sigmoid(g)
    return o, (removed, v, decay, taken, added)


def write_state(parts, state_ref, at_rows, spread_ref):
    removed, v, decay, taken, added = parts
    rows, head = v.shape
    flat = state_ref.shape[1]
    chunk = 8 * head
    pair = jnp.concatenate([removed, v], axis=0)
    high = pair.astype(jnp.bfloat16)
    low = (pair - high.astype(jnp.float32)).astype(jnp.bfloat16)
    pair = jnp.concatenate([high, low], axis=1)
    decay_w, taken_w, added_w = [lanes(t, chunk // head) for t in (decay, taken, added)]
    for at in range(0, flat, chunk):
        wide = jnp.dot(pair, spread_ref[:, at : at + chunk], preferred_element_type=jnp.float32)
        state_ref[at_rows, at : at + chunk] = (
            state_ref[at_rows, at : at + chunk] * decay_w
            - wide[:rows] * taken_w
            + wide[rows:] * added_w
        )


def fused_kernel(n, own_ref, gain_ref, bias_ref, self_ref, ro_ref, spread_ref, *refs):
    weights, (w_out, state, mixed_ref, new_ref), refs = refs[:6], refs[6:10], refs[10:]
    full_ref, next_ref, joined_ref, wo_ref, o_out, o_in, z_out, z_in, fin, fin_in, mine, *sems = refs
    load, g_send, g_recv_a, g_recv_b, w_send, w_recv, o_send, o_recv, z_send, z_recv, f_send, f_recv = sems
    layers = state.shape[0]
    head = weights[0].shape[2]
    rows, columns = own_ref.shape
    block = columns // 8
    deep = 8 * rows
    f32, bf16 = jnp.float32, jnp.bfloat16

    loads = [[], []]
    state_loads = []
    for layer in range(layers):
        for i, w in enumerate(weights):
            copy = pltpu.make_async_copy(
                w.at[layer, 0], joined_ref.at[layer, pl.ds(i * head, head)], load.at[layer, i]
            )
            copy.start()
            loads[layer].append(copy)
        copy = pltpu.make_async_copy(state.at[layer, 0], new_ref.at[layer, 0], load.at[layer, 6])
        copy.start()
        state_loads.append(copy)

    at = Place(n)
    at.greet()
    own_cols = pl.ds(pl.multiple_of(at.i * block, block), block)
    own_slot = pl.ds(pl.multiple_of(at.i * head, head), head)
    sent = []

    def share_weights(layer):
        for s, to in enumerate(at.others):
            cols = pl.ds(pl.multiple_of(to % 8 * block, block), block)
            copy = remote(
                w_out.at[layer, 0, :, cols],
                wo_ref.at[layer, own_slot],
                w_send.at[layer, s],
                w_recv.at[layer, at.i],
                to,
            )
            copy.start()
            sent.append(copy)
        copy = pltpu.make_async_copy(
            w_out.at[layer, 0, :, own_cols], wo_ref.at[layer, own_slot], load.at[layer, 7]
        )
        copy.start()
        return copy

    def weights_here(layer, own_copy):
        own_copy.wait()
        for other in at.others:
            slot = wo_ref.at[layer, pl.ds(pl.multiple_of(other % 8 * head, head), head)]
            remote(slot, slot, w_send.at[layer, 0], w_recv.at[layer, other % 8], at.sib).wait_recv()

    def mixer(layer, gather, reads, after_last):
        heads = [own_head(t, layer, head) for t in (bias_ref, self_ref, ro_ref)]
        layer_state = new_ref.at[layer, 0]
        waited = []

        def batch(k):
            if not waited:
                for copy in loads[layer]:
                    copy.wait()
                state_loads[layer].wait()
                waited.append(1)
            p = at.plane(k)
            here = pl.ds(pl.multiple_of(p * deep, deep), deep)
            proj = project(layer, functools.partial(reads, p), columns, gain_ref, joined_ref)
            o, parts = read_state(proj, heads, layer_state, here, spread_ref)
            packed = jnp.concatenate([o[: deep // 2], o[deep // 2 :]], axis=1).astype(bf16)
            o_out[layer, k] = packed
            o_in[layer, k, at.i] = packed
            for s, to in enumerate(at.others):
                copy = remote(
                    o_out.at[layer, k],
                    o_in.at[layer, k, at.i],
                    o_send.at[layer, k, s],
                    o_recv.at[layer, k, at.i],
                    to,
                )
                copy.start()
                sent.append(copy)
            write_state(parts, layer_state, here, spread_ref)

        gather.run(batch)
        own_copy = after_last()
        weights_here(layer, own_copy)
        for k in gather.order:
            for other in at.others:
                slot = o_in.at[layer, k, other % 8]
                remote(
                    slot, slot, o_send.at[layer, k, 0], o_recv.at[layer, k, other % 8], at.sib
                ).wait_recv()
            tops, bottoms = [], []
            for j in range(8):
                got = o_in[layer, k, j]
                tops.append(got[:, :head])
                bottoms.append(got[:, head:])
            left = jnp.concatenate(
                [jnp.concatenate(tops, axis=1), jnp.concatenate(bottoms, axis=1)], axis=0
            )
            part = jnp.dot(left, wo_ref[layer], preferred_element_type=f32)
            if k:
                z_out[layer, k] = part.astype(bf16)
                copy = remote(
                    z_out.at[layer, k], z_in.at[layer, k], z_send.at[layer, k], z_recv.at[layer, k], at.zn(k)
                )
                copy.start()
                sent.append(copy)
            else:
                mine[...] = part
        total = mine[...]
        for k in at.near:
            slot = z_in.at[layer, k]
            remote(slot, slot, z_send.at[layer, k], z_recv.at[layer, k], at.sib).wait_recv()
            total = total + z_in[layer, k].astype(f32)
        return total

    full_ref[at.me] = own_ref[...]
    first = Gather(at, own_ref, full_ref, g_send.at[0], g_recv_a.at[0], g_recv_b.at[0])
    first.start()

    def first_reads(p, j):
        tiles = pl.ds(pl.multiple_of(p * 8, 8), 8)
        return full_ref[tiles, :, j * block : (j + 1) * block].reshape(deep, block)

    held = []

    def after_first():
        held.append(share_weights(1))
        return held[0]

    w0 = share_weights(0)
    total = mixer(0, first, first_reads, lambda: (held.append(share_weights(1)), w0)[1])
    mine_tiles = pl.ds(pl.multiple_of(at.z * 8, 8), 8)
    resid = full_ref[mine_tiles, :, own_cols].reshape(deep, block).astype(f32)
    piece = (resid + total).astype(bf16)
    next_ref[at.me] = piece
    second = Gather(at, next_ref.at[at.me], next_ref, g_send.at[1], g_recv_a.at[1], g_recv_b.at[1])
    second.start()
    total = mixer(1, second, lambda p, j: next_ref[p * 8 + j], lambda: held[0])
    done = (next_ref[at.me].astype(f32) + total).astype(bf16)
    fin[...] = done.reshape(8, rows, block)
    fin_in[at.i] = fin[at.i]
    for s, to in enumerate(at.others):
        copy = remote(fin.at[to % 8], fin_in.at[at.i], f_send.at[s], f_recv.at[at.i], to)
        copy.start()
        sent.append(copy)
    for other in at.others:
        slot = fin_in.at[other % 8]
        remote(slot, slot, f_send.at[0], f_recv.at[other % 8], at.sib).wait_recv()
    for j in range(8):
        mixed_ref[:, j * block : (j + 1) * block] = fin_in[j]
    first.drain()
    second.drain()
    for copy in sent:
        copy.wait_send()


def on_device_fast(n, *args):
    tokens, gain, wr, wk, wv, wd, wq, wg, bias, self_w, ro_gain, w_out, state = args
    weights = [jnp.swapaxes(w, 2, 3) for w in (wr, wk, wv, wd, wq, wg)]
    own = tokens[0]
    rows, columns = own.shape
    head = wr.shape[3]
    layers = state.shape[0]
    flat = state.shape[3]
    planes = n // 8
    block, deep = columns // 8, 8 * rows
    bf16, f32 = jnp.bfloat16, jnp.float32
    value_of = jnp.arange(flat) // head
    spread = (jnp.arange(2 * head)[:, None] % head == value_of[None]).astype(bf16)
    vmem, hbm = [pl.BlockSpec(memory_space=m) for m in (pltpu.VMEM, pltpu.HBM)]
    dma = pltpu.SemaphoreType.DMA
    mixed, new_state = pl.pallas_call(
        functools.partial(fused_kernel, n),
        out_shape=(
            jax.ShapeDtypeStruct(own.shape, own.dtype),
            jax.ShapeDtypeStruct(state.shape, state.dtype),
        ),
        in_specs=[vmem] * 6 + [hbm] * 8,
        out_specs=(vmem, vmem),
        scratch_shapes=[
            pltpu.VMEM((n, rows, columns), bf16),
            pltpu.VMEM((n, deep, block), bf16),
            pltpu.VMEM((layers, 6 * head, columns), bf16),
            pltpu.VMEM((layers, 8 * head, block), bf16),
            pltpu.VMEM((layers, planes, deep // 2, 2 * head), bf16),
            pltpu.VMEM((layers, planes, 8, deep // 2, 2 * head), bf16),
            pltpu.VMEM((layers, planes, deep, block), bf16),
            pltpu.VMEM((layers, planes, deep, block), bf16),
            pltpu.VMEM((8, rows, block), bf16),
            pltpu.VMEM((8, rows, block), bf16),
            pltpu.VMEM((deep, block), f32),
            dma((layers, 8)),
            dma((layers, gather_sends(n))),
            dma((layers, n)),
            dma((layers, n)),
            dma((layers, 7)),
            dma((layers, 8)),
            dma((layers, planes, 7)),
            dma((layers, planes, 8)),
            dma((layers, planes)),
            dma((layers, planes)),
            dma((7,)),
            dma((8,)),
        ],
        compiler_params=pltpu.CompilerParams(
            collective_id=0, has_side_effects=True, vmem_limit_bytes=40 << 20
        ),
        cost_estimate=pl.CostEstimate(flops=0, bytes_accessed=50 << 20, transcendentals=0),
    )(own, gain, bias, self_w, ro_gain, spread, *weights, w_out, state)
    return mixed[None], new_state


def pick(n, *args):
    one_block = args[0].shape[2] == args[1].shape[1]
    tiles = args[0].shape[1] % 8 == 0 and args[0].shape[2] % 1024 == 0
    if one_block and tiles and n % 16 == 0 and 2 * args[2].shape[3] % 128 == 0:
        return on_device_fast(n, *args)
    return on_device(*args)


def solution(mesh):
    return jax.shard_map(
        functools.partial(pick, mesh.shape["tp"]),
        mesh=mesh,
        in_specs=(
            P("tp", None, None),
            P(),
            P(None, "tp", None, None),
            P(None, "tp", None, None),
            P(None, "tp", None, None),
            P(None, "tp", None, None),
            P(None, "tp", None, None),
            P(None, "tp", None, None),
            P(),
            P(),
            P(),
            P(None, "tp", None, None),
            P(None, "tp", None, None),
        ),
        out_specs=(P("tp", None, None), P(None, "tp", None, None)),
        check_vma=False,
    )
```

time: 106 us -> 112 us (1.057); the launches traced: 106 us -> 111 us
  local copies, waits for them, and re-layouts: 3.97 us -> 20.7 us
  Pallas kernels: 101 us -> 89.3 us
    unnamed x17 -> x26, local copies, waits for them, and re-layouts: 3.97 us -> 20.7 us
    pallas_call x5 -> x1, Pallas kernels: 101 us -> 89.3 us  [on_device_fast(): pl.pallas_call(functools.partial(fused_kernel, n), out_shape=(jax.ShapeDt...]
where the time goes in v1:
time: 112 us; the launch traced here: 111 us
  Pallas kernels  89.3 us (80%)
  local copies, waits for them, and re-layouts  20.7 us (18%)
    pallas_call x1, Pallas kernels, on_device_fast(): pl.pallas_call(functools.partial(fused_kernel, n), out_shape=(jax.ShapeDt...  89.3 us
    unnamed x26, local copies, waits for them, and re-layouts  20.7 us

profile of v1, /device:TPU:0, one launch (start us, length us, event | category | flops | bytes accessed | tf_op | source)
XLA Modules:
  0.0 111.0 jit_solution(17733925860470964548)
XLA Ops:
  0.7 0.3 compare_convert_fusion.spread_ref
  0.9 0.0 copy-start
  0.9 1.2 %copy-done = bf16[2,1,4096,64]{2,3,1,0:T(8,128)(2,1)S(1)} copy-done((bf16[2,1,4096,64]{2,3,1,0:T(8,128)(2,1)S(1)}, bf16[2,1,4096,64]{2,3,1,0:T(8,128)(2,1)}, u32[]{:S(2)}) %copy-start) | copy-done | bytes 1048600
  2.1 0.0 copy-start.1
  2.1 1.2 %copy-done.1 = bf16[2,1,4096,64]{2,3,1,0:T(8,128)(2,1)S(1)} copy-done((bf16[2,1,4096,64]{2,3,1,0:T(8,128)(2,1)S(1)}, bf16[2,1,4096,64]{2,3,1,0:T(8,128)(2,1)}, u32[]{:S(2)}) %copy-start.1) | copy-done | bytes 1048600
  3.4 0.0 copy-start.2
  3.4 1.2 %copy-done.2 = bf16[2,1,4096,64]{2,3,1,0:T(8,128)(2,1)S(1)} copy-done((bf16[2,1,4096,64]{2,3,1,0:T(8,128)(2,1)S(1)}, bf16[2,1,4096,64]{2,3,1,0:T(8,128)(2,1)}, u32[]{:S(2)}) %copy-start.2) | copy-done | bytes 1048600
  4.6 0.0 copy-start.3
  4.6 1.2 %copy-done.3 = bf16[2,1,4096,64]{2,3,1,0:T(8,128)(2,1)S(1)} copy-done((bf16[2,1,4096,64]{2,3,1,0:T(8,128)(2,1)S(1)}, bf16[2,1,4096,64]{2,3,1,0:T(8,128)(2,1)}, u32[]{:S(2)}) %copy-start.3) | copy-done | bytes 1048600
  5.8 0.0 copy-start.4
  5.8 1.2 %copy-done.4 = bf16[2,1,4096,64]{2,3,1,0:T(8,128)(2,1)S(1)} copy-done((bf16[2,1,4096,64]{2,3,1,0:T(8,128)(2,1)S(1)}, bf16[2,1,4096,64]{2,3,1,0:T(8,128)(2,1)}, u32[]{:S(2)}) %copy-start.4) | copy-done | bytes 1048600
  7.0 0.0 copy-start.5
  7.0 1.2 %copy-done.5 = bf16[2,1,4096,64]{2,3,1,0:T(8,128)(2,1)S(1)} copy-done((bf16[2,1,4096,64]{2,3,1,0:T(8,128)(2,1)S(1)}, bf16[2,1,4096,64]{2,3,1,0:T(8,128)(2,1)}, u32[]{:S(2)}) %copy-start.5) | copy-done | bytes 1048600
  8.3 0.0 copy-start.6
  8.3 1.2 %copy-done.6 = bf16[2,1,64,4096]{3,2,1,0:T(8,128)(2,1)S(1)} copy-done((bf16[2,1,64,4096]{3,2,1,0:T(8,128)(2,1)S(1)}, bf16[2,1,64,4096]{3,2,1,0:T(8,128)(2,1)}, u32[]{:S(2)}) %copy-start.6) | copy-done | bytes 1048600
  9.5 0.0 copy-start.7
  9.5 0.8 copy-done.7
  10.3 0.0 copy-start.8
  10.3 0.8 copy-done.8
  11.1 0.0 copy-start.9
  11.1 0.7 copy-done.9
  11.8 0.0 copy-start.10
  11.8 0.7 copy-done.10
  12.5 0.0 copy-start.11
  12.5 0.7 copy-done.11
  13.2 89.3 %shard_map.140 = (bf16[8,4096]{1,0:T(8,128)(2,1)S(1)}, f32[2,1,256,4096]{3,2,1,0:T(8,128)}) custom-call(bf16[8,4096]{1,0:T(8,128)(2,1)S(1)} %bitcast.14, f32[2,4096]{1,0:T(2,128)S(1)} %copy-done.8, f32[2,2048]{1,0:T(2,128)S(1)} %copy-done.9, f32[2,2048]{1,0:T(2,128)S(1)} %copy-done.10, f32[2,2048]{1,0:T(2,128)S(1)} %copy-done.11, ...), custom_call_target="tpu_custom_call" | custom-call | bytes 52428800 | tf_op jit(solution)/shard_map/pallas_call | solution.py:603
  102.6 0.6 copy.17
  103.2 7.8 %copy.18 = f32[2,1,256,4096]{3,2,1,0:T(8,128)} copy(f32[2,1,256,4096]{3,2,1,0:T(8,128)} %get-tuple-element.9) | data formatting | bytes 16777216
  (2 shorter events, 0.0 us)
Async XLA Ops:
  0.9 1.2 %copy-start = (bf16[2,1,4096,64]{2,3,1,0:T(8,128)(2,1)S(1)}, bf16[2,1,4096,64]{2,3,1,0:T(8,128)(2,1)}, u32[]{:S(2)}) copy-start(bf16[2,1,4096,64]{2,3,1,0:T(8,128)(2,1)} %param.15) | copy-start | bytes 3145732
  2.1 1.2 %copy-start.1 = (bf16[2,1,4096,64]{2,3,1,0:T(8,128)(2,1)S(1)}, bf16[2,1,4096,64]{2,3,1,0:T(8,128)(2,1)}, u32[]{:S(2)}) copy-start(bf16[2,1,4096,64]{2,3,1,0:T(8,128)(2,1)} %param.16) | copy-start | bytes 3145732
  3.4 1.2 %copy-start.2 = (bf16[2,1,4096,64]{2,3,1,0:T(8,128)(2,1)S(1)}, bf16[2,1,4096,64]{2,3,1,0:T(8,128)(2,1)}, u32[]{:S(2)}) copy-start(bf16[2,1,4096,64]{2,3,1,0:T(8,128)(2,1)} %param.17) | copy-start | bytes 3145732
  4.6 1.2 %copy-start.3 = (bf16[2,1,4096,64]{2,3,1,0:T(8,128)(2,1)S(1)}, bf16[2,1,4096,64]{2,3,1,0:T(8,128)(2,1)}, u32[]{:S(2)}) copy-start(bf16[2,1,4096,64]{2,3,1,0:T(8,128)(2,1)} %param.18) | copy-start | bytes 3145732
  5.8 1.2 %copy-start.4 = (bf16[2,1,4096,64]{2,3,1,0:T(8,128)(2,1)S(1)}, bf16[2,1,4096,64]{2,3,1,0:T(8,128)(2,1)}, u32[]{:S(2)}) copy-start(bf16[2,1,4096,64]{2,3,1,0:T(8,128)(2,1)} %param.19) | copy-start | bytes 3145732
  7.0 1.2 %copy-start.5 = (bf16[2,1,4096,64]{2,3,1,0:T(8,128)(2,1)S(1)}, bf16[2,1,4096,64]{2,3,1,0:T(8,128)(2,1)}, u32[]{:S(2)}) copy-start(bf16[2,1,4096,64]{2,3,1,0:T(8,128)(2,1)} %param.20) | copy-start | bytes 3145732
  8.3 1.2 %copy-start.6 = (bf16[2,1,64,4096]{3,2,1,0:T(8,128)(2,1)S(1)}, bf16[2,1,64,4096]{3,2,1,0:T(8,128)(2,1)}, u32[]{:S(2)}) copy-start(bf16[2,1,64,4096]{3,2,1,0:T(8,128)(2,1)} %refs_6_.1) | copy-start | bytes 3145732
  9.5 0.8 copy-start.7
  10.3 0.8 copy-start.8
  11.1 0.7 copy-start.9
  11.8 0.7 copy-start.10
  12.5 0.7 copy-start.11

commit v2 on v1

--- a/solution.py
+++ b/solution.py
@@ -201,8 +201,8 @@
         self.yn = self.peer(1, 0, 0)
         flips = [(1, 1, 0), (1, 1, 1), (1, 0, 0), (1, 0, 1), (0, 1, 0), (0, 1, 1), (0, 0, 1)]
         self.others = [self.peer(*f) for f in flips]
-        half = self.planes // 2
-        self.near = [k for k in range(1, self.planes) if k != half] + [half]
+        self.xyn = self.others[0]
+        self.near = list(range(1, self.planes))
 
     def peer(self, dy, dx, dc):
         flip = lambda v, d: 1 - v if d else v
@@ -212,7 +212,8 @@
         return ((p * 2 + y) * 2 + x) * 2 + c
 
     def plane(self, k):
-        return (self.z + k) % self.planes
+        low, high = self.z % 2, self.z // 2
+        return 2 * (1 - high if k // 2 else high) + (1 - low if k % 2 else low)
 
     def zn(self, k):
         return self.plane(k) * 8 + self.i
@@ -240,96 +241,54 @@
 
 def gather_sends(n):
     planes = n // 8
-    return (planes - 1) + 3 * planes + 4 * planes + 2 * planes
+    return (planes - 1) + 7 * planes
 
 
 class Gather:
-    def __init__(self, at, own_ref, full_ref, send, recv_a, recv_b):
+    def __init__(self, at, own_ref, full_ref, send, recv):
         self.at, self.own, self.full = at, own_ref, full_ref
-        self.send, self.recv_a, self.recv_b = send, recv_a, recv_b
-        half = full_ref.shape[2] // 2
-        self.first, self.second = pl.ds(0, half), pl.ds(half, half)
+        self.send, self.recv = send, recv
         self.started = []
-        self.order = [0] + at.near
-
-    def go(self, src, t, to, cols=None, recv=None):
+
+    def go(self, src, t, *tos):
+        for to in tos:
+            sem = self.send.at[len(self.started)]
+            copy = remote(src, self.full.at[t], sem, self.recv.at[t], to)
+            copy.start()
+            self.started.append(copy)
+
+    def arrived(self, t):
         dst = self.full.at[t]
-        if cols is not None:
-            src, dst = src.at[:, cols], dst.at[:, cols]
-        recv = self.recv_a if recv is None else recv
-        copy = remote(src, dst, self.send.at[len(self.started)], recv.at[t], to)
-        copy.start()
-        self.started.append(copy)
-
-    def arrived(self, t, cols=None, recv=None):
-        dst = self.full.at[t]
-        if cols is not None:
-            dst = dst.at[:, cols]
-        recv = self.recv_a if recv is None else recv
-        remote(dst, dst, self.send.at[0], recv.at[t], self.at.sib).wait_recv()
+        remote(dst, dst, self.send.at[0], self.recv.at[t], self.at.sib).wait_recv()
 
     def start(self):
         at = self.at
         for k in at.near:
             self.go(self.own, at.me, at.zn(k))
-        self.go(self.own, at.me, at.xn)
-        self.go(self.own, at.me, at.yn)
-        self.go(self.own, at.me, at.sib)
+        self.go(self.own, at.me, at.xyn, at.xn, at.yn, at.sib)
 
     def column(self, k):
         at = self.at
         t = at.zn(k)
         self.arrived(t)
-        for to in (at.xn, at.yn, at.sib):
-            self.go(self.full.at[t], t, to)
-
-    def spread(self, k):
+        self.go(self.full.at[t], t, at.xyn, at.xn, at.yn, at.sib)
+
+    def across(self, k, c):
         at = self.at
         p = at.plane(k)
-        t = at.tile(p, at.y, 1 - at.x, at.c)
-        self.arrived(t)
-        self.go(self.full.at[t], t, at.yn, self.first, self.recv_a)
-        self.go(self.full.at[t], t, at.sib)
-        t = at.tile(p, 1 - at.y, at.x, at.c)
-        self.arrived(t)
-        self.go(self.full.at[t], t, at.xn, self.second, self.recv_b)
-        self.go(self.full.at[t], t, at.sib)
-
-    def corner(self, k):
-        at = self.at
-        t = at.tile(at.plane(k), 1 - at.y, 1 - at.x, at.c)
-        self.arrived(t, self.first, self.recv_a)
-        self.go(self.full.at[t], t, at.sib, self.first, self.recv_a)
-        self.arrived(t, self.second, self.recv_b)
-        self.go(self.full.at[t], t, at.sib, self.second, self.recv_b)
+        spots = ((at.y, 1 - at.x), (1 - at.y, at.x), (1 - at.y, 1 - at.x))
+        return [at.tile(p, y, x, c) for y, x in spots]
+
+    def sides(self, k):
+        for t in self.across(k, self.at.c):
+            self.arrived(t)
+            self.go(self.full.at[t], t, self.at.sib)
 
     def finish(self, k):
         at = self.at
-        p = at.plane(k)
-        for y in (at.y, 1 - at.y):
-            for x in (at.x, 1 - at.x):
-                t = at.tile(p, y, x, 1 - at.c)
-                if y is not at.y and x is not at.x:
-                    self.arrived(t, self.first, self.recv_a)
-                    self.arrived(t, self.second, self.recv_b)
-                else:
-                    self.arrived(t)
-
-    def run(self, batch):
-        order = self.order
-        for step, k in enumerate(order):
-            if step:
-                self.column(k)
-                self.spread(order[step - 1])
-            if step >= 2:
-                self.corner(order[step - 2])
-        self.spread(order[-1])
-        if len(order) > 1:
-            self.corner(order[-2])
-        self.corner(order[-1])
-        for k in order:
-            self.finish(k)
-            batch(k)
+        self.arrived(at.tile(at.plane(k), at.y, at.x, 1 - at.c))
+        for t in self.across(k, 1 - at.c):
+            self.arrived(t)
 
     def drain(self):
         for copy in self.started:
@@ -426,18 +385,42 @@
         )
 
 
-def fused_kernel(n, own_ref, gain_ref, bias_ref, self_ref, ro_ref, spread_ref, *refs):
+def put_spread(spread_ref, head):
+    chunk = 8 * head
+    shape = (spread_ref.shape[0], chunk)
+    lane = lax.broadcasted_iota(jnp.int32, shape, 1) // head
+    row = lax.broadcasted_iota(jnp.int32, shape, 0) % head
+    for at in range(0, spread_ref.shape[1], chunk):
+        hit = row == lane + at // head
+        spread_ref[:, at : at + chunk] = jnp.where(hit, 1.0, 0.0).astype(jnp.bfloat16)
+
+
+def fused_kernel(n, own_hbm, gain_hbm, bias_hbm, self_hbm, ro_hbm, *refs):
     weights, (w_out, state, mixed_ref, new_ref), refs = refs[:6], refs[6:10], refs[10:]
+    spread_ref, gain_ref, bias_ref, self_ref, ro_ref, early, *refs = refs
     full_ref, next_ref, joined_ref, wo_ref, o_out, o_in, z_out, z_in, fin, fin_in, mine, *sems = refs
-    load, g_send, g_recv_a, g_recv_b, w_send, w_recv, o_send, o_recv, z_send, z_recv, f_send, f_recv = sems
+    load, g_send, g_recv, w_send, w_recv, o_send, o_recv, z_send, z_recv, f_send, f_recv = sems
     layers = state.shape[0]
     head = weights[0].shape[2]
-    rows, columns = own_ref.shape
+    rows, columns = own_hbm.shape
     block = columns // 8
     deep = 8 * rows
     f32, bf16 = jnp.float32, jnp.bfloat16
-
-    loads = [[], []]
+    at = Place(n)
+
+    def fetch(i, src, dst):
+        copy = pltpu.make_async_copy(src, dst, early.at[i])
+        copy.start()
+        return copy
+
+    own_load = fetch(0, own_hbm, full_ref.at[at.me])
+    tables = [
+        fetch(1, gain_hbm, gain_ref),
+        fetch(2, bias_hbm, bias_ref),
+        fetch(3, self_hbm, self_ref),
+        fetch(4, ro_hbm, ro_ref),
+    ]
+    loads = [tables] + [[] for _ in range(1, layers)]
     state_loads = []
     for layer in range(layers):
         for i, w in enumerate(weights):
@@ -450,11 +433,10 @@
         copy.start()
         state_loads.append(copy)
 
-    at = Place(n)
     at.greet()
     own_cols = pl.ds(pl.multiple_of(at.i * block, block), block)
     own_slot = pl.ds(pl.multiple_of(at.i * head, head), head)
-    sent = []
+    sent, own_weights = [], []
 
     def share_weights(layer):
         for s, to in enumerate(at.others):
@@ -472,29 +454,37 @@
             w_out.at[layer, 0, :, own_cols], wo_ref.at[layer, own_slot], load.at[layer, 7]
         )
         copy.start()
-        return copy
-
-    def weights_here(layer, own_copy):
-        own_copy.wait()
+        own_weights.append(copy)
+
+    def weights_here(layer):
+        own_weights[layer].wait()
         for other in at.others:
             slot = wo_ref.at[layer, pl.ds(pl.multiple_of(other % 8 * head, head), head)]
             remote(slot, slot, w_send.at[layer, 0], w_recv.at[layer, other % 8], at.sib).wait_recv()
 
-    def mixer(layer, gather, reads, after_last):
-        heads = [own_head(t, layer, head) for t in (bias_ref, self_ref, ro_ref)]
+    def mixer(layer, gather, reads, share_early, share_late):
+        heads = []
         layer_state = new_ref.at[layer, 0]
-        waited = []
-
-        def batch(k):
-            if not waited:
+        zero, a, b, c = range(at.planes)
+        held = {}
+
+        def here(k):
+            return pl.ds(pl.multiple_of(at.plane(k) * deep, deep), deep)
+
+        def projected(k):
+            gather.finish(k)
+            if not heads:
                 for copy in loads[layer]:
                     copy.wait()
+                heads.extend(own_head(t, layer, head) for t in (bias_ref, self_ref, ro_ref))
+            held[k] = project(
+                layer, functools.partial(reads, at.plane(k)), columns, gain_ref, joined_ref
+            )
+
+        def mixed_rows(k):
+            if k == zero:
                 state_loads[layer].wait()
-                waited.append(1)
-            p = at.plane(k)
-            here = pl.ds(pl.multiple_of(p * deep, deep), deep)
-            proj = project(layer, functools.partial(reads, p), columns, gain_ref, joined_ref)
-            o, parts = read_state(proj, heads, layer_state, here, spread_ref)
+            o, held[k] = read_state(held[k], heads, layer_state, here(k), spread_ref)
             packed = jnp.concatenate([o[: deep // 2], o[deep // 2 :]], axis=1).astype(bf16)
             o_out[layer, k] = packed
             o_in[layer, k, at.i] = packed
@@ -508,12 +498,11 @@
                 )
                 copy.start()
                 sent.append(copy)
-            write_state(parts, layer_state, here, spread_ref)
-
-        gather.run(batch)
-        own_copy = after_last()
-        weights_here(layer, own_copy)
-        for k in gather.order:
+
+        def update(k):
+            write_state(held[k], layer_state, here(k), spread_ref)
+
+        def emit(k):
             for other in at.others:
                 slot = o_in.at[layer, k, other % 8]
                 remote(
@@ -528,15 +517,42 @@
                 [jnp.concatenate(tops, axis=1), jnp.concatenate(bottoms, axis=1)], axis=0
             )
             part = jnp.dot(left, wo_ref[layer], preferred_element_type=f32)
-            if k:
-                z_out[layer, k] = part.astype(bf16)
-                copy = remote(
-                    z_out.at[layer, k], z_in.at[layer, k], z_send.at[layer, k], z_recv.at[layer, k], at.zn(k)
-                )
-                copy.start()
-                sent.append(copy)
-            else:
+            if k == zero:
                 mine[...] = part
+                return
+            z_out[layer, k] = part.astype(bf16)
+            copy = remote(
+                z_out.at[layer, k], z_in.at[layer, k], z_send.at[layer, k], z_recv.at[layer, k], at.zn(k)
+            )
+            copy.start()
+            sent.append(copy)
+
+        gather.column(a)
+        gather.sides(zero)
+        gather.column(b)
+        projected(zero)
+        gather.column(c)
+        share_early()
+        gather.sides(a)
+        mixed_rows(zero)
+        projected(a)
+        gather.sides(b)
+        mixed_rows(a)
+        gather.sides(c)
+        projected(b)
+        mixed_rows(b)
+        projected(c)
+        mixed_rows(c)
+        share_late()
+        update(zero)
+        weights_here(layer)
+        emit(a)
+        emit(b)
+        emit(zero)
+        update(a)
+        update(b)
+        emit(c)
+        update(c)
         total = mine[...]
         for k in at.near:
             slot = z_in.at[layer, k]
@@ -544,29 +560,26 @@
             total = total + z_in[layer, k].astype(f32)
         return total
 
-    full_ref[at.me] = own_ref[...]
-    first = Gather(at, own_ref, full_ref, g_send.at[0], g_recv_a.at[0], g_recv_b.at[0])
+    own_load.wait()
+    first = Gather(at, full_ref.at[at.me], full_ref, g_send.at[0], g_recv.at[0])
     first.start()
 
     def first_reads(p, j):
         tiles = pl.ds(pl.multiple_of(p * 8, 8), 8)
         return full_ref[tiles, :, j * block : (j + 1) * block].reshape(deep, block)
 
-    held = []
-
-    def after_first():
-        held.append(share_weights(1))
-        return held[0]
-
-    w0 = share_weights(0)
-    total = mixer(0, first, first_reads, lambda: (held.append(share_weights(1)), w0)[1])
+    put_spread(spread_ref, head)
+    total = mixer(
+        0, first, first_reads, functools.partial(share_weights, 0), functools.partial(share_weights, 1)
+    )
     mine_tiles = pl.ds(pl.multiple_of(at.z * 8, 8), 8)
     resid = full_ref[mine_tiles, :, own_cols].reshape(deep, block).astype(f32)
     piece = (resid + total).astype(bf16)
     next_ref[at.me] = piece
-    second = Gather(at, next_ref.at[at.me], next_ref, g_send.at[1], g_recv_a.at[1], g_recv_b.at[1])
+    second = Gather(at, next_ref.at[at.me], next_ref, g_send.at[1], g_recv.at[1])
     second.start()
-    total = mixer(1, second, lambda p, j: next_ref[p * 8 + j], lambda: held[0])
+    nothing = lambda: None
+    total = mixer(1, second, lambda p, j: next_ref[p * 8 + j], nothing, nothing)
     done = (next_ref[at.me].astype(f32) + total).astype(bf16)
     fin[...] = done.reshape(8, rows, block)
     fin_in[at.i] = fin[at.i]
@@ -596,19 +609,22 @@
     planes = n // 8
     block, deep = columns // 8, 8 * rows
     bf16, f32 = jnp.bfloat16, jnp.float32
-    value_of = jnp.arange(flat) // head
-    spread = (jnp.arange(2 * head)[:, None] % head == value_of[None]).astype(bf16)
     vmem, hbm = [pl.BlockSpec(memory_space=m) for m in (pltpu.VMEM, pltpu.HBM)]
     dma = pltpu.SemaphoreType.DMA
+    stay = lambda a: pltpu.with_memory_space_constraint(a, pltpu.HBM)
+    operands = [own, gain, bias, self_w, ro_gain, *weights, w_out, state]
     mixed, new_state = pl.pallas_call(
         functools.partial(fused_kernel, n),
         out_shape=(
             jax.ShapeDtypeStruct(own.shape, own.dtype),
-            jax.ShapeDtypeStruct(state.shape, state.dtype),
+            pltpu.VMEM(state.shape, state.dtype),
         ),
-        in_specs=[vmem] * 6 + [hbm] * 8,
+        in_specs=[hbm] * len(operands),
         out_specs=(vmem, vmem),
         scratch_shapes=[
+            pltpu.VMEM((2 * head, flat), bf16),
+            *[pltpu.VMEM(t.shape, t.dtype) for t in (gain, bias, self_w, ro_gain)],
+            dma((5,)),
             pltpu.VMEM((n, rows, columns), bf16),
             pltpu.VMEM((n, deep, block), bf16),
             pltpu.VMEM((layers, 6 * head, columns), bf16),
@@ -623,7 +639,6 @@
             dma((layers, 8)),
             dma((layers, gather_sends(n))),
             dma((layers, n)),
-            dma((layers, n)),
             dma((layers, 7)),
             dma((layers, 8)),
             dma((layers, planes, 7)),
@@ -637,14 +652,14 @@
             collective_id=0, has_side_effects=True, vmem_limit_bytes=40 << 20
         ),
         cost_estimate=pl.CostEstimate(flops=0, bytes_accessed=50 << 20, transcendentals=0),
-    )(own, gain, bias, self_w, ro_gain, spread, *weights, w_out, state)
+    )(*[stay(o) for o in operands])
     return mixed[None], new_state
 
 
 def pick(n, *args):
     one_block = args[0].shape[2] == args[1].shape[1]
     tiles = args[0].shape[1] % 8 == 0 and args[0].shape[2] % 1024 == 0
-    if one_block and tiles and n % 16 == 0 and 2 * args[2].shape[3] % 128 == 0:
+    if one_block and tiles and n // 8 == 4 and 2 * args[2].shape[3] % 128 == 0:
         return on_device_fast(n, *args)
     return on_device(*args)
 

time: 112 us -> 76.1 us (0.68)
  Pallas kernels: 89.3 us -> 71.3 us
  local copies, waits for them, and re-layouts: 20.7 us -> 4.03 us
    pallas_call x1, Pallas kernels: 89.3 us -> 71.3 us  [on_device_fast(): pl.pallas_call(functools.partial(fused_kernel, n), out_shape=(jax.ShapeDt...]
    unnamed x26 -> x2, local copies, waits for them, and re-layouts: 20.7 us -> 4.03 us
where the time goes in v2:
time: 76.1 us; the launch traced here: 76 us
  Pallas kernels  71.3 us (94%)
  local copies, waits for them, and re-layouts  4.03 us (5%)
    pallas_call x1, Pallas kernels, on_device_fast(): pl.pallas_call(functools.partial(fused_kernel, n), out_shape=(jax.ShapeDt...  71.3 us
    unnamed x2, local copies, waits for them, and re-layouts  4.03 us

profile of v2, /device:TPU:0, one launch (start us, length us, event | category | flops | bytes accessed | tf_op | source)
XLA Modules:
  0.0 76.0 jit_solution(7993761738903445686)
XLA Ops:
  0.6 71.3 %shard_map.140 = (bf16[8,4096]{1,0:T(8,128)(2,1)S(1)}, f32[2,1,256,4096]{3,2,1,0:T(8,128)S(1)}) custom-call(bf16[8,4096]{1,0:T(8,128)(2,1)} %bitcast.15, f32[2,4096]{1,0:T(2,128)} %gain_hbm.1, f32[2,2048]{1,0:T(2,128)} %bias_hbm.1, f32[2,2048]{1,0:T(2,128)} %self_hbm.1, f32[2,2048]{1,0:T(2,128)} %ro_hbm.1, bf16[2,1,64,4096]{3,2,1,0:T(8,128)(2,1)} %bitcast.9, ...), custom_call_target="tpu_custom_call" | custom-call | bytes 52428800 | tf_op jit(solution)/shard_map/pallas_call | solution.py:616
  71.9 3.4 %copy.17 = f32[2,1,256,4096]{3,2,1,0:T(8,128)} copy(f32[2,1,256,4096]{3,2,1,0:T(8,128)S(1)} %get-tuple-element.7) | data formatting | bytes 16777216
  75.3 0.6 copy.18

commit v3 on v2

--- a/solution.py
+++ b/solution.py
@@ -202,7 +202,7 @@
         flips = [(1, 1, 0), (1, 1, 1), (1, 0, 0), (1, 0, 1), (0, 1, 0), (0, 1, 1), (0, 0, 1)]
         self.others = [self.peer(*f) for f in flips]
         self.xyn = self.others[0]
-        self.near = list(range(1, self.planes))
+        self.near = [1, 3, 2]
 
     def peer(self, dy, dx, dc):
         flip = lambda v, d: 1 - v if d else v
@@ -239,60 +239,90 @@
     )
 
 
-def gather_sends(n):
-    planes = n // 8
-    return (planes - 1) + 7 * planes
+GATHER_SENDS = 3 + 4 + 1 + 2 * 4 + 6 + 3 * 3
 
 
 class Gather:
     def __init__(self, at, own_ref, full_ref, send, recv):
         self.at, self.own, self.full = at, own_ref, full_ref
         self.send, self.recv = send, recv
-        self.started = []
-
-    def go(self, src, t, *tos):
+        self.inner = at.z % 2 != at.z // 2
+
+    def spot(self, k, i):
+        return k * 4 + i
+
+    def go(self, src, t, spot, *tos):
         for to in tos:
-            sem = self.send.at[len(self.started)]
-            copy = remote(src, self.full.at[t], sem, self.recv.at[t], to)
-            copy.start()
-            self.started.append(copy)
-
-    def arrived(self, t):
-        dst = self.full.at[t]
-        remote(dst, dst, self.send.at[0], self.recv.at[t], self.at.sib).wait_recv()
+            remote(src, self.full.at[t], self.send.at[0], self.recv.at[spot], to).start()
+
+    def arrived(self, spot, tiles=1):
+        dst = self.full.at[pl.ds(0, tiles)]
+        remote(dst, dst, self.send.at[0], self.recv.at[spot], self.at.sib).wait_recv()
+
+    def cross(self, k, src, t):
+        at = self.at
+        for i, to in enumerate((at.xyn, at.xn, at.yn)):
+            self.go(src, t, self.spot(k, i), to)
+        self.to_sib(k, src, t)
+
+    def to_sib(self, k, src, t):
+        self.go(src, t, self.spot(k, 3), self.at.sib)
+
+    def along(self, k):
+        return 4 * self.at.planes + k - 1
 
     def start(self):
         at = self.at
-        for k in at.near:
-            self.go(self.own, at.me, at.zn(k))
-        self.go(self.own, at.me, at.xyn, at.xn, at.yn, at.sib)
+        for k in (1, 3):
+            self.go(self.own, at.me, self.along(k), at.zn(k))
+
+        @pl.when(jnp.logical_not(self.inner))
+        def _():
+            self.go(self.own, at.me, self.along(2), at.zn(2))
+
+        self.cross(0, self.own, at.me)
+
+    def adjacent(self):
+        t = self.at.zn(1)
+        self.arrived(self.along(1))
+        self.to_sib(1, self.full.at[t], t)
 
     def column(self, k):
-        at = self.at
-        t = at.zn(k)
-        self.arrived(t)
-        self.go(self.full.at[t], t, at.xyn, at.xn, at.yn, at.sib)
-
-    def across(self, k, c):
+        t = self.at.zn(k)
+        self.arrived(self.along(k))
+        self.cross(k, self.full.at[t], t)
+
+    def middle_early(self):
+        @pl.when(self.inner)
+        def _():
+            t = self.at.zn(3)
+            self.arrived(self.along(3))
+            self.go(self.full.at[t], t, self.along(2), self.at.zn(1))
+            self.cross(3, self.full.at[t], t)
+
+    def middle_late(self):
+        @pl.when(jnp.logical_not(self.inner))
+        def _():
+            self.column(3)
+
+    def sides(self, k):
         at = self.at
         p = at.plane(k)
-        spots = ((at.y, 1 - at.x), (1 - at.y, at.x), (1 - at.y, 1 - at.x))
-        return [at.tile(p, y, x, c) for y, x in spots]
-
-    def sides(self, k):
-        for t in self.across(k, self.at.c):
-            self.arrived(t)
-            self.go(self.full.at[t], t, self.at.sib)
+        spots = ((1 - at.y, 1 - at.x), (at.y, 1 - at.x), (1 - at.y, at.x))
+        for i in (1, 2, 0):
+            y, x = spots[i]
+            t = at.tile(p, y, x, at.c)
+            self.arrived(self.spot(k, i))
+            if not k:
+                self.go(self.full.at[t], t, self.spot(1, i), at.zn(1))
+            self.to_sib(k, self.full.at[t], t)
 
     def finish(self, k):
-        at = self.at
-        self.arrived(at.tile(at.plane(k), at.y, at.x, 1 - at.c))
-        for t in self.across(k, 1 - at.c):
-            self.arrived(t)
+        self.arrived(self.spot(k, 3), 4)
 
     def drain(self):
-        for copy in self.started:
-            copy.wait_send()
+        dst = self.full.at[pl.ds(0, GATHER_SENDS)]
+        remote(dst, dst, self.send.at[0], self.recv.at[0], self.at.sib).wait_send()
 
 
 def lanes(v, times):
@@ -420,52 +450,49 @@
         fetch(3, self_hbm, self_ref),
         fetch(4, ro_hbm, ro_ref),
     ]
-    loads = [tables] + [[] for _ in range(1, layers)]
     state_loads = []
-    for layer in range(layers):
-        for i, w in enumerate(weights):
-            copy = pltpu.make_async_copy(
-                w.at[layer, 0], joined_ref.at[layer, pl.ds(i * head, head)], load.at[layer, i]
-            )
+    def load_bulk():
+        for layer in range(layers):
+            for i, w in enumerate(weights):
+                copy = pltpu.make_async_copy(
+                    w.at[layer, 0], joined_ref.at[layer, pl.ds(i * head, head)], load.at[layer, 0]
+                )
+                copy.start()
+            copy = pltpu.make_async_copy(state.at[layer, 0], new_ref.at[layer, 0], load.at[layer, 1])
             copy.start()
-            loads[layer].append(copy)
-        copy = pltpu.make_async_copy(state.at[layer, 0], new_ref.at[layer, 0], load.at[layer, 6])
-        copy.start()
-        state_loads.append(copy)
+            state_loads.append(copy)
 
     at.greet()
     own_cols = pl.ds(pl.multiple_of(at.i * block, block), block)
     own_slot = pl.ds(pl.multiple_of(at.i * head, head), head)
-    sent, own_weights = [], []
+    own_weights = []
 
     def share_weights(layer):
-        for s, to in enumerate(at.others):
+        for to in at.others:
             cols = pl.ds(pl.multiple_of(to % 8 * block, block), block)
             copy = remote(
                 w_out.at[layer, 0, :, cols],
                 wo_ref.at[layer, own_slot],
-                w_send.at[layer, s],
-                w_recv.at[layer, at.i],
+                w_send.at[layer],
+                w_recv.at[layer],
                 to,
             )
             copy.start()
-            sent.append(copy)
         copy = pltpu.make_async_copy(
-            w_out.at[layer, 0, :, own_cols], wo_ref.at[layer, own_slot], load.at[layer, 7]
+            w_out.at[layer, 0, :, own_cols], wo_ref.at[layer, own_slot], load.at[layer, 2]
         )
         copy.start()
         own_weights.append(copy)
 
     def weights_here(layer):
         own_weights[layer].wait()
-        for other in at.others:
-            slot = wo_ref.at[layer, pl.ds(pl.multiple_of(other % 8 * head, head), head)]
-            remote(slot, slot, w_send.at[layer, 0], w_recv.at[layer, other % 8], at.sib).wait_recv()
+        slots = wo_ref.at[layer, pl.ds(0, 7 * head)]
+        remote(slots, slots, w_send.at[layer], w_recv.at[layer], at.sib).wait()
 
     def mixer(layer, gather, reads, share_early, share_late):
         heads = []
         layer_state = new_ref.at[layer, 0]
-        zero, a, b, c = range(at.planes)
+        zero, a, b, c = [0] + at.near
         held = {}
 
         def here(k):
@@ -474,8 +501,11 @@
         def projected(k):
             gather.finish(k)
             if not heads:
-                for copy in loads[layer]:
-                    copy.wait()
+                if not layer:
+                    for copy in tables:
+                        copy.wait()
+                whole = joined_ref.at[layer]
+                pltpu.make_async_copy(whole, whole, load.at[layer, 0]).wait()
                 heads.extend(own_head(t, layer, head) for t in (bias_ref, self_ref, ro_ref))
             held[k] = project(
                 layer, functools.partial(reads, at.plane(k)), columns, gain_ref, joined_ref
@@ -488,26 +518,17 @@
             packed = jnp.concatenate([o[: deep // 2], o[deep // 2 :]], axis=1).astype(bf16)
             o_out[layer, k] = packed
             o_in[layer, k, at.i] = packed
-            for s, to in enumerate(at.others):
-                copy = remote(
-                    o_out.at[layer, k],
-                    o_in.at[layer, k, at.i],
-                    o_send.at[layer, k, s],
-                    o_recv.at[layer, k, at.i],
-                    to,
-                )
-                copy.start()
-                sent.append(copy)
+            for to in at.others:
+                remote(
+                    o_out.at[layer, k], o_in.at[layer, k, at.i], o_send.at[k], o_recv.at[k], to
+                ).start()
 
         def update(k):
             write_state(held[k], layer_state, here(k), spread_ref)
 
         def emit(k):
-            for other in at.others:
-                slot = o_in.at[layer, k, other % 8]
-                remote(
-                    slot, slot, o_send.at[layer, k, 0], o_recv.at[layer, k, other % 8], at.sib
-                ).wait_recv()
+            slots = o_in.at[layer, k, pl.ds(0, 7)]
+            remote(slots, slots, o_send.at[k], o_recv.at[k], at.sib).wait()
             tops, bottoms = [], []
             for j in range(8):
                 got = o_in[layer, k, j]
@@ -521,48 +542,48 @@
                 mine[...] = part
                 return
             z_out[layer, k] = part.astype(bf16)
-            copy = remote(
-                z_out.at[layer, k], z_in.at[layer, k], z_send.at[layer, k], z_recv.at[layer, k], at.zn(k)
-            )
-            copy.start()
-            sent.append(copy)
-
-        gather.column(a)
+            remote(
+                z_out.at[layer, k], z_in.at[layer, k], z_send.at[layer], z_recv.at[layer], at.zn(k)
+            ).start()
+
+        gather.middle_early()
+        gather.adjacent()
         gather.sides(zero)
-        gather.column(b)
-        projected(zero)
+        gather.middle_late()
         gather.column(c)
         share_early()
+        projected(zero)
+        mixed_rows(zero)
         gather.sides(a)
-        mixed_rows(zero)
         projected(a)
         gather.sides(b)
         mixed_rows(a)
+        projected(b)
         gather.sides(c)
-        projected(b)
         mixed_rows(b)
         projected(c)
         mixed_rows(c)
-        share_late()
-        update(zero)
         weights_here(layer)
         emit(a)
+        emit(zero)
         emit(b)
-        emit(zero)
+        update(zero)
         update(a)
+        emit(c)
+        share_late()
         update(b)
-        emit(c)
         update(c)
         total = mine[...]
+        slots = z_in.at[layer, pl.ds(1, at.planes - 1)]
+        remote(slots, slots, z_send.at[layer], z_recv.at[layer], at.sib).wait()
         for k in at.near:
-            slot = z_in.at[layer, k]
-            remote(slot, slot, z_send.at[layer, k], z_recv.at[layer, k], at.sib).wait_recv()
             total = total + z_in[layer, k].astype(f32)
         return total
 
     own_load.wait()
-    first = Gather(at, full_ref.at[at.me], full_ref, g_send.at[0], g_recv.at[0])
+    first = Gather(at, full_ref.at[at.me], full_ref, g_send, g_recv)
     first.start()
+    load_bulk()
 
     def first_reads(p, j):
         tiles = pl.ds(pl.multiple_of(p * 8, 8), 8)
@@ -575,27 +596,42 @@
     mine_tiles = pl.ds(pl.multiple_of(at.z * 8, 8), 8)
     resid = full_ref[mine_tiles, :, own_cols].reshape(deep, block).astype(f32)
     piece = (resid + total).astype(bf16)
+    first.drain()
     next_ref[at.me] = piece
-    second = Gather(at, next_ref.at[at.me], next_ref, g_send.at[1], g_recv.at[1])
+    second = Gather(at, next_ref.at[at.me], next_ref, g_send, g_recv)
     second.start()
     nothing = lambda: None
     total = mixer(1, second, lambda p, j: next_ref[p * 8 + j], nothing, nothing)
     done = (next_ref[at.me].astype(f32) + total).astype(bf16)
     fin[...] = done.reshape(8, rows, block)
     fin_in[at.i] = fin[at.i]
-    for s, to in enumerate(at.others):
-        copy = remote(fin.at[to % 8], fin_in.at[at.i], f_send.at[s], f_recv.at[at.i], to)
-        copy.start()
-        sent.append(copy)
-    for other in at.others:
-        slot = fin_in.at[other % 8]
-        remote(slot, slot, f_send.at[0], f_recv.at[other % 8], at.sib).wait_recv()
+    for to in at.others:
+        remote(fin.at[to % 8], fin_in.at[at.i], f_send.at[0], f_recv.at[0], to).start()
+    slots = fin_in.at[pl.ds(0, 7)]
+    remote(slots, slots, f_send.at[0], f_recv.at[0], at.sib).wait()
     for j in range(8):
         mixed_ref[:, j * block : (j + 1) * block] = fin_in[j]
-    first.drain()
     second.drain()
-    for copy in sent:
-        copy.wait_send()
+
+
+WRITES = 4
+
+
+def write_kernel(mixed_ref, state_ref, mixed_hbm, state_hbm, done):
+    copies = [pltpu.make_async_copy(mixed_ref, mixed_hbm, done.at[0])]
+    layers, _, rows, _ = state_ref.shape
+    for layer in range(layers):
+        for part in range(WRITES):
+            here = pl.ds(part * (rows // WRITES), rows // WRITES)
+            copies.append(
+                pltpu.make_async_copy(
+                    state_ref.at[layer, 0, here], state_hbm.at[layer, 0, here], done.at[len(copies)]
+                )
+            )
+    for copy in copies:
+        copy.start()
+    for copy in copies:
+        copy.wait()
 
 
 def on_device_fast(n, *args):
@@ -616,7 +652,7 @@
     mixed, new_state = pl.pallas_call(
         functools.partial(fused_kernel, n),
         out_shape=(
-            jax.ShapeDtypeStruct(own.shape, own.dtype),
+            pltpu.VMEM(own.shape, own.dtype),
             pltpu.VMEM(state.shape, state.dtype),
         ),
         in_specs=[hbm] * len(operands),
@@ -636,23 +672,32 @@
             pltpu.VMEM((8, rows, block), bf16),
             pltpu.VMEM((8, rows, block), bf16),
             pltpu.VMEM((deep, block), f32),
-            dma((layers, 8)),
-            dma((layers, gather_sends(n))),
-            dma((layers, n)),
-            dma((layers, 7)),
-            dma((layers, 8)),
-            dma((layers, planes, 7)),
-            dma((layers, planes, 8)),
-            dma((layers, planes)),
-            dma((layers, planes)),
-            dma((7,)),
-            dma((8,)),
+            dma((layers, 3)),
+            dma((1,)),
+            dma((5 * planes - 1,)),
+            dma((layers,)),
+            dma((layers,)),
+            dma((planes,)),
+            dma((planes,)),
+            dma((layers,)),
+            dma((layers,)),
+            dma((1,)),
+            dma((1,)),
         ],
         compiler_params=pltpu.CompilerParams(
             collective_id=0, has_side_effects=True, vmem_limit_bytes=40 << 20
         ),
         cost_estimate=pl.CostEstimate(flops=0, bytes_accessed=50 << 20, transcendentals=0),
     )(*[stay(o) for o in operands])
+    held = [pltpu.with_memory_space_constraint(a, pltpu.VMEM) for a in (mixed, new_state)]
+    mixed, new_state = pl.pallas_call(
+        write_kernel,
+        out_shape=[jax.ShapeDtypeStruct(a.shape, a.dtype) for a in held],
+        in_specs=[vmem, vmem],
+        out_specs=[hbm, hbm],
+        scratch_shapes=[dma((1 + WRITES * layers,))],
+        compiler_params=pltpu.CompilerParams(vmem_limit_bytes=1 << 20),
+    )(*held)
     return mixed[None], new_state
 
 

time: 76.1 us -> 69.5 us (0.913)
  local copies, waits for them, and re-layouts: 4.03 us -> 0 us
  Pallas kernels: 71.3 us -> 68.7 us
    unnamed x2 -> x0, local copies, waits for them, and re-layouts: 4.03 us -> none
    pallas_call x1 -> x2, Pallas kernels: 71.3 us -> 68.7 us  [the longest x1 65.3 us: on_device_fast(): pl.pallas_call(functools.partial(fused_kernel, n), out_shape=(pltpu.VMEM(...]
where the time goes in v3:
time: 69.5 us; the launch traced here: 69.4 us
  Pallas kernels  68.7 us (99%)
    pallas_call x1, Pallas kernels, on_device_fast(): pl.pallas_call(functools.partial(fused_kernel, n), out_shape=(pltpu.VMEM(...  65.3 us
    pallas_call x1, Pallas kernels, on_device_fast(): pl.pallas_call(write_kernel, out_shape=[jax.ShapeDtypeStruct(a.shape, a.d...  3.4 us

profile of v3, /device:TPU:0, one launch (start us, length us, event | category | flops | bytes accessed | tf_op | source)
XLA Modules:
  0.0 69.4 jit_solution(4613586361916279277)
XLA Ops:
  0.6 65.3 %shard_map.140 = (bf16[8,4096]{1,0:T(8,128)(2,1)S(1)}, f32[2,1,256,4096]{3,2,1,0:T(8,128)S(1)}) custom-call(bf16[8,4096]{1,0:T(8,128)(2,1)} %bitcast.14, f32[2,4096]{1,0:T(2,128)} %gain_hbm.1, f32[2,2048]{1,0:T(2,128)} %bias_hbm.1, f32[2,2048]{1,0:T(2,128)} %self_hbm.1, f32[2,2048]{1,0:T(2,128)} %ro_hbm.1, bf16[2,1,64,4096]{3,2,1,0:T(8,128)(2,1)} %bitcast.8, ...), custom_call_target="tpu_custom_call" | custom-call | bytes 52428800 | tf_op jit(solution)/shard_map/pallas_call | solution.py:652
  66.0 3.4 %shard_map.141 = (bf16[8,4096]{1,0:T(8,128)(2,1)}, f32[2,1,256,4096]{3,2,1,0:T(8,128)}) custom-call(bf16[8,4096]{1,0:T(8,128)(2,1)S(1)} %get-tuple-element.6.mixed_ref, f32[2,1,256,4096]{3,2,1,0:T(8,128)S(1)} %get-tuple-element.7.state_ref), custom_call_target="tpu_custom_call" | custom-call | tf_op jit(solution)/shard_map/pallas_call | solution.py:693

commit v4 on v3

--- a/solution.py
+++ b/solution.py
@@ -261,8 +261,9 @@
 
     def cross(self, k, src, t):
         at = self.at
-        for i, to in enumerate((at.xyn, at.xn, at.yn)):
-            self.go(src, t, self.spot(k, i), to)
+        tos = (at.xyn, at.xn, at.yn)
+        for i in (0, 1, 2) if k else (1, 2, 0):
+            self.go(src, t, self.spot(k, i), tos[i])
         self.to_sib(k, src, t)
 
     def to_sib(self, k, src, t):
@@ -285,6 +286,7 @@
     def adjacent(self):
         t = self.at.zn(1)
         self.arrived(self.along(1))
+        self.go(self.full.at[t], t, self.spot(1, 0), self.at.xyn)
         self.to_sib(1, self.full.at[t], t)
 
     def column(self, k):
@@ -313,7 +315,7 @@
             y, x = spots[i]
             t = at.tile(p, y, x, at.c)
             self.arrived(self.spot(k, i))
-            if not k:
+            if not k and i:
                 self.go(self.full.at[t], t, self.spot(1, i), at.zn(1))
             self.to_sib(k, self.full.at[t], t)
 
@@ -538,6 +540,15 @@
                 [jnp.concatenate(tops, axis=1), jnp.concatenate(bottoms, axis=1)], axis=0
             )
             part = jnp.dot(left, wo_ref[layer], preferred_element_type=f32)
+            if layer == layers - 1:
+                fin[k] = part.astype(bf16).reshape(8, rows, block)
+                if k == zero:
+                    fin_in[k * 8 + at.i] = fin[k, at.i]
+                for to in at.others if k == zero else [at.plane(k) * 8 + j for j in range(8)]:
+                    remote(
+                        fin.at[k, to % 8], fin_in.at[k * 8 + at.i], f_send.at[0], f_recv.at[0], to
+                    ).start()
+                return
             if k == zero:
                 mine[...] = part
                 return
@@ -573,6 +584,8 @@
         share_late()
         update(b)
         update(c)
+        if layer == layers - 1:
+            return None
         total = mine[...]
         slots = z_in.at[layer, pl.ds(1, at.planes - 1)]
         remote(slots, slots, z_send.at[layer], z_recv.at[layer], at.sib).wait()
@@ -597,20 +610,19 @@
     resid = full_ref[mine_tiles, :, own_cols].reshape(deep, block).astype(f32)
     piece = (resid + total).astype(bf16)
     first.drain()
-    next_ref[at.me] = piece
+    next_ref[at.me] = piece.reshape(8, rows, block)
     second = Gather(at, next_ref.at[at.me], next_ref, g_send, g_recv)
     second.start()
     nothing = lambda: None
-    total = mixer(1, second, lambda p, j: next_ref[p * 8 + j], nothing, nothing)
-    done = (next_ref[at.me].astype(f32) + total).astype(bf16)
-    fin[...] = done.reshape(8, rows, block)
-    fin_in[at.i] = fin[at.i]
-    for to in at.others:
-        remote(fin.at[to % 8], fin_in.at[at.i], f_send.at[0], f_recv.at[0], to).start()
-    slots = fin_in.at[pl.ds(0, 7)]
+    second_reads = lambda p, j: next_ref[p * 8 + j].reshape(deep, block)
+    mixer(1, second, second_reads, nothing, nothing)
+    slots = fin_in.at[pl.ds(0, n - 1)]
     remote(slots, slots, f_send.at[0], f_recv.at[0], at.sib).wait()
     for j in range(8):
-        mixed_ref[:, j * block : (j + 1) * block] = fin_in[j]
+        tile = next_ref[at.z * 8 + j, at.i].astype(f32)
+        for k in range(at.planes):
+            tile = tile + fin_in[k * 8 + j].astype(f32)
+        mixed_ref[:, j * block : (j + 1) * block] = tile.astype(bf16)
     second.drain()
 
 
@@ -662,15 +674,15 @@
             *[pltpu.VMEM(t.shape, t.dtype) for t in (gain, bias, self_w, ro_gain)],
             dma((5,)),
             pltpu.VMEM((n, rows, columns), bf16),
-            pltpu.VMEM((n, deep, block), bf16),
+            pltpu.VMEM((n, 8, rows, block), bf16),
             pltpu.VMEM((layers, 6 * head, columns), bf16),
             pltpu.VMEM((layers, 8 * head, block), bf16),
             pltpu.VMEM((layers, planes, deep // 2, 2 * head), bf16),
             pltpu.VMEM((layers, planes, 8, deep // 2, 2 * head), bf16),
             pltpu.VMEM((layers, planes, deep, block), bf16),
             pltpu.VMEM((layers, planes, deep, block), bf16),
-            pltpu.VMEM((8, rows, block), bf16),
-            pltpu.VMEM((8, rows, block), bf16),
+            pltpu.VMEM((planes, 8, rows, block), bf16),
+            pltpu.VMEM((n, rows, block), bf16),
             pltpu.VMEM((deep, block), f32),
             dma((layers, 3)),
             dma((1,)),

time: 69.5 us -> 66.1 us (0.951)
  Pallas kernels: 68.7 us -> 65.3 us
    pallas_call x1, Pallas kernels: 65.3 us -> 61.9 us  [on_device_fast(): pl.pallas_call(functools.partial(fused_kernel, n), out_shape=(pltpu.VMEM(...]
where the time goes in v4:
time: 66.1 us; the launch traced here: 66 us
  Pallas kernels  65.3 us (99%)
    pallas_call x1, Pallas kernels, on_device_fast(): pl.pallas_call(functools.partial(fused_kernel, n), out_shape=(pltpu.VMEM(...  61.9 us
    pallas_call x1, Pallas kernels, on_device_fast(): pl.pallas_call(write_kernel, out_shape=[jax.ShapeDtypeStruct(a.shape, a.d...  3.4 us

profile of v4, /device:TPU:0, one launch (start us, length us, event | category | flops | bytes accessed | tf_op | source)
XLA Modules:
  0.0 66.0 jit_solution(16000153306852061964)
XLA Ops:
  0.6 61.9 %shard_map.140 = (bf16[8,4096]{1,0:T(8,128)(2,1)S(1)}, f32[2,1,256,4096]{3,2,1,0:T(8,128)S(1)}) custom-call(bf16[8,4096]{1,0:T(8,128)(2,1)} %bitcast.14, f32[2,4096]{1,0:T(2,128)} %gain_hbm.1, f32[2,2048]{1,0:T(2,128)} %bias_hbm.1, f32[2,2048]{1,0:T(2,128)} %self_hbm.1, f32[2,2048]{1,0:T(2,128)} %ro_hbm.1, bf16[2,1,64,4096]{3,2,1,0:T(8,128)(2,1)} %bitcast.8, ...), custom_call_target="tpu_custom_call" | custom-call | bytes 52428800 | tf_op jit(solution)/shard_map/pallas_call | solution.py:664
  62.6 3.4 %shard_map.141 = (bf16[8,4096]{1,0:T(8,128)(2,1)}, f32[2,1,256,4096]{3,2,1,0:T(8,128)}) custom-call(bf16[8,4096]{1,0:T(8,128)(2,1)S(1)} %get-tuple-element.6.mixed_ref, f32[2,1,256,4096]{3,2,1,0:T(8,128)S(1)} %get-tuple-element.7.state_ref), custom_call_target="tpu_custom_call" | custom-call | tf_op jit(solution)/shard_map/pallas_call | solution.py:705

commit v5 on v4

--- a/solution.py
+++ b/solution.py
@@ -307,11 +307,11 @@
         def _():
             self.column(3)
 
-    def sides(self, k):
+    def sides(self, k, which=(1, 2, 0)):
         at = self.at
         p = at.plane(k)
         spots = ((1 - at.y, 1 - at.x), (at.y, 1 - at.x), (1 - at.y, at.x))
-        for i in (1, 2, 0):
+        for i in which:
             y, x = spots[i]
             t = at.tile(p, y, x, at.c)
             self.arrived(self.spot(k, i))
@@ -362,6 +362,7 @@
 
 
 def read_state(proj, heads, state_ref, at_rows, spread_ref):
+    take = lambda cols: [state_ref[here, cols] for here in at_rows]
     bias, self_w, ro_gain = heads
     head = bias.shape[1]
     rows = proj.shape[0]
@@ -375,7 +376,7 @@
     kn_w, u_w = lanes(kn, chunk // head), lanes(decay * r, chunk // head)
     sums = jnp.zeros((2 * rows, head), jnp.float32)
     for at in range(0, flat, chunk):
-        s = state_ref[at_rows, at : at + chunk]
+        s = jnp.concatenate(take(slice(at, at + chunk)), axis=0)
         both = jnp.concatenate([s * kn_w, s * u_w], axis=0).astype(jnp.bfloat16)
         sums += lax.dot_general(
             both,
@@ -500,8 +501,9 @@
         def here(k):
             return pl.ds(pl.multiple_of(at.plane(k) * deep, deep), deep)
 
-        def projected(k):
-            gather.finish(k)
+        def projected(*ks):
+            for k in ks:
+                gather.finish(k)
             if not heads:
                 if not layer:
                     for copy in tables:
@@ -509,21 +511,25 @@
                 whole = joined_ref.at[layer]
                 pltpu.make_async_copy(whole, whole, load.at[layer, 0]).wait()
                 heads.extend(own_head(t, layer, head) for t in (bias_ref, self_ref, ro_ref))
-            held[k] = project(
-                layer, functools.partial(reads, at.plane(k)), columns, gain_ref, joined_ref
-            )
-
-        def mixed_rows(k):
-            if k == zero:
+            read = lambda j: jnp.concatenate([reads(at.plane(k), j) for k in ks], axis=0)
+            held[ks] = project(layer, read, columns, gain_ref, joined_ref)
+
+        def mixed_rows(*ks):
+            if zero in ks:
                 state_loads[layer].wait()
-            o, held[k] = read_state(held[k], heads, layer_state, here(k), spread_ref)
-            packed = jnp.concatenate([o[: deep // 2], o[deep // 2 :]], axis=1).astype(bf16)
-            o_out[layer, k] = packed
-            o_in[layer, k, at.i] = packed
-            for to in at.others:
-                remote(
-                    o_out.at[layer, k], o_in.at[layer, k, at.i], o_send.at[k], o_recv.at[k], to
-                ).start()
+            rows_of = [here(k) for k in ks]
+            o, parts = read_state(held[ks], heads, layer_state, rows_of, spread_ref)
+            for m, k in enumerate(ks):
+                cut = lambda t: t[m * deep : (m + 1) * deep]
+                held[k] = [cut(t) for t in parts]
+                top, bottom = cut(o)[: deep // 2], cut(o)[deep // 2 :]
+                packed = jnp.concatenate([top, bottom], axis=1).astype(bf16)
+                o_out[layer, k] = packed
+                o_in[layer, k, at.i] = packed
+                for to in at.others:
+                    remote(
+                        o_out.at[layer, k], o_in.at[layer, k, at.i], o_send.at[k], o_recv.at[k], to
+                    ).start()
 
         def update(k):
             write_state(held[k], layer_state, here(k), spread_ref)
@@ -559,25 +565,24 @@
 
         gather.middle_early()
         gather.adjacent()
-        gather.sides(zero)
+        gather.sides(zero, (1, 2))
         gather.middle_late()
+        gather.sides(zero, (0,))
         gather.column(c)
-        share_early()
         projected(zero)
         mixed_rows(zero)
         gather.sides(a)
-        projected(a)
         gather.sides(b)
-        mixed_rows(a)
-        projected(b)
+        share_early()
+        projected(a, b)
         gather.sides(c)
-        mixed_rows(b)
+        mixed_rows(a, b)
         projected(c)
         mixed_rows(c)
         weights_here(layer)
+        emit(b)
         emit(a)
         emit(zero)
-        emit(b)
         update(zero)
         update(a)
         emit(c)

time: 66.1 us -> 63.6 us (0.962)
  Pallas kernels: 65.3 us -> 62.5 us
    pallas_call x1, Pallas kernels: 61.9 us -> 59.1 us  [on_device_fast(): pl.pallas_call(functools.partial(fused_kernel, n), out_shape=(pltpu.VMEM(...]
where the time goes in v5:
time: 63.6 us; the launch traced here: 63.2 us
  Pallas kernels  62.5 us (98%)
  between operations  0.64 us (1%)
    pallas_call x1, Pallas kernels, on_device_fast(): pl.pallas_call(functools.partial(fused_kernel, n), out_shape=(pltpu.VMEM(...  59.1 us
    pallas_call x1, Pallas kernels, on_device_fast(): pl.pallas_call(write_kernel, out_shape=[jax.ShapeDtypeStruct(a.shape, a.d...  3.4 us

profile of v5, /device:TPU:0, one launch (start us, length us, event | category | flops | bytes accessed | tf_op | source)
XLA Modules:
  0.0 63.2 jit_solution(6180907311246650940)
XLA Ops:
  0.6 59.1 %shard_map.140 = (bf16[8,4096]{1,0:T(8,128)(2,1)S(1)}, f32[2,1,256,4096]{3,2,1,0:T(8,128)S(1)}) custom-call(bf16[8,4096]{1,0:T(8,128)(2,1)} %bitcast.14, f32[2,4096]{1,0:T(2,128)} %gain_hbm.1, f32[2,2048]{1,0:T(2,128)} %bias_hbm.1, f32[2,2048]{1,0:T(2,128)} %self_hbm.1, f32[2,2048]{1,0:T(2,128)} %ro_hbm.1, bf16[2,1,64,4096]{3,2,1,0:T(8,128)(2,1)} %bitcast.8, ...), custom_call_target="tpu_custom_call" | custom-call | bytes 52428800 | tf_op jit(solution)/shard_map/pallas_call | solution.py:669
  59.8 3.4 %shard_map.141 = (bf16[8,4096]{1,0:T(8,128)(2,1)}, f32[2,1,256,4096]{3,2,1,0:T(8,128)}) custom-call(bf16[8,4096]{1,0:T(8,128)(2,1)S(1)} %get-tuple-element.6.mixed_ref, f32[2,1,256,4096]{3,2,1,0:T(8,128)S(1)} %get-tuple-element.7.state_ref), custom_call_target="tpu_custom_call" | custom-call | tf_op jit(solution)/shard_map/pallas_call | solution.py:710
